TPU v7x, 32 devices: a whole 2x2x4 slice. The times are simulated.
32 devices in a mesh: sp: 16 (over z, y, core), tp: 2 (over x).
Axes of the slice: x: 2, y: 2, z: 4, core: 2. Of those that a mesh axis runs over, the one named last changes fastest.
Arguments:
- query_latent: bfloat16 [4096, 1024], P('sp'), may hold values from -6 to 6
- shared_latent: bfloat16 [4096, 512], P('sp'), may hold values from -25 to 25
- rotary_key: bfloat16 [4096, 64], P('sp'), may hold values from -300 to 300
- document_start: int32 [4096], P('sp'), may hold values from 0 to 4095, as said below
- query_gain: float32 [1024], replicated, may hold values from 0.1 to 1.9
- shared_gain: float32 [512], replicated, may hold values from 0.1 to 1.9
- content_weight: bfloat16 [1024, 2048], P(None, 'tp'), may hold values from -0.1875 to 0.1875
- rotary_weight: bfloat16 [1024, 1024], P(None, 'tp'), may hold values from -0.1875 to 0.1875
- key_weight: bfloat16 [512, 2048], P(None, 'tp'), may hold values from -0.25 to 0.25
- value_weight: bfloat16 [512, 2048], P(None, 'tp'), may hold values from -0.25 to 0.25
- output_weight: bfloat16 [2048, 4096], P('tp'), may hold values from -0.125 to 0.125
Outputs:
- mixed: bfloat16 [4096, 4096], P('sp')
Inputs may be any that keep to these rules, and one draw needn't show every extreme that they name: `document_start`: each position holds the first position of its document; documents are runs of 1 to 1792 consecutive positions and one of them has exactly 1792; the values never fall.
All inputs are finite; a program needn't handle non-finite values.
Results may differ from a plain program's by a relative error of at most 0.038.
The roundings to bfloat16 on the way count: a program that leaves them out, or rounds other values in their place, can miss the bound.
Values may be sent and summed in bfloat16 or wider, within the bound.
No kernel may reach another device: no remote copies, remote signals or barrier semaphores. Data moves between devices by JAX's collectives and lax.ppermute only.
A program may use at most 64 MiB of HBM per device.

v0:
```python
import functools

import jax
import jax.numpy as jnp
from jax import lax
from jax.experimental import pallas as pl
from jax.experimental.pallas import tpu as pltpu
from jax.sharding import PartitionSpec as P

CONTENT = 128
ROTARY = 64
VALUE_DIM = 128
GROUP = 4

norm_eps = 1e-06
rope_theta = 10000.0
masked_score = -1e30
LOG2E = 1.4426950408889634


def vmem():
    return pl.BlockSpec(memory_space=pltpu.VMEM)


def grant(mebibytes):
    return pltpu.CompilerParams(vmem_limit_bytes=mebibytes * 2**20)


def smem():
    return pl.BlockSpec(memory_space=pltpu.SMEM)


def normed(latent, gain):
    entries = latent.astype(jnp.float32)
    scale = lax.rsqrt(jnp.mean(entries * entries, axis=-1, keepdims=True) + norm_eps)
    return (entries * scale * gain).astype(jnp.bfloat16)


def swap_halves(x):
    width = x.shape[-1]
    half = ROTARY // 2
    lane = lax.broadcasted_iota(jnp.int32, x.shape, x.ndim - 1)
    ahead = pltpu.roll(x, width - half, x.ndim - 1)
    behind = pltpu.roll(x, half, x.ndim - 1)
    return jnp.where(lane % ROTARY < half, ahead, behind)


def pack_kernel(shared_ref, rotary_ref, gain_ref, cos_ref, sin_ref, out_ref):
    length, rank = shared_ref.shape
    out_ref[0:length, :] = normed(shared_ref[...], gain_ref[...])
    key = rotary_ref[...].astype(jnp.float32)
    key = jnp.concatenate([key, key], axis=-1)
    turned = key * cos_ref[...] + swap_halves(key) * sin_ref[...]
    rows = length * ROTARY // rank
    lane = lax.broadcasted_iota(jnp.int32, (rows, 2 * ROTARY), 1)
    for pair in range(rank // (2 * ROTARY)):
        low = turned[(2 * pair) * rows : (2 * pair + 1) * rows]
        high = turned[(2 * pair + 1) * rows : (2 * pair + 2) * rows]
        out_ref[length:, pair * 2 * ROTARY : (pair + 1) * 2 * ROTARY] = jnp.where(
            lane < ROTARY, low, high
        ).astype(jnp.bfloat16)


def query_kernel(latent_ref, gain_ref, content_ref, rotary_ref, cos_ref, sin_ref, out_ref):
    rows = normed(latent_ref[...], gain_ref[...])
    content = jnp.dot(rows, content_ref[...], preferred_element_type=jnp.float32)
    raw = jnp.dot(rows, rotary_ref[...], preferred_element_type=jnp.float32)
    lane = lax.broadcasted_iota(jnp.int32, (rows.shape[0], 2 * ROTARY), 1)
    for pair in range(out_ref.shape[0] // 2):
        piece = raw[:, pair * 2 * ROTARY : (pair + 1) * 2 * ROTARY]
        turned = piece * cos_ref[...] + swap_halves(piece) * sin_ref[...]
        for side in range(2):
            head = 2 * pair + side
            out_ref[head, :, 0:CONTENT] = content[
                :, head * CONTENT : (head + 1) * CONTENT
            ].astype(jnp.bfloat16)
            own = (lane < ROTARY) if side == 0 else (lane >= ROTARY)
            out_ref[head, :, CONTENT:] = jnp.where(own, turned, 0.0).astype(jnp.bfloat16)


def attend_kernel(places, axis, first, *refs):
    count = len(places)
    starts_smem, starts_ref, query_ref, key_ref, value_ref = refs[:5]
    blocks = refs[5 : 5 + count]
    refs = refs[5 + count :]
    if not first:
        old_stat, old_acc = refs[:2]
        refs = refs[2:]
    stat_ref, acc_ref, bias_ref, keys_ref, values_ref = refs
    heads = query_ref.shape[0]
    length = query_ref.shape[1]
    rank = key_ref.shape[0]
    me = lax.axis_index(axis)
    first_start = starts_smem[0]
    scale = (CONTENT + ROTARY) ** (-0.5) * LOG2E
    if not first:
        stat_ref[...] = old_stat[...]
        acc_ref[...] = old_acc[...]

    def process(place_of, block_ref, own):
        block = place_of(me)

        def work():
            shared = block_ref[0:length, :]
            keys_ref[...] = jnp.dot(
                shared, key_ref[...], preferred_element_type=jnp.float32
            ).astype(jnp.bfloat16)
            values_ref[...] = lax.dot_general(
                value_ref[...], shared, (((1,), (1,)), ((), ())), preferred_element_type=jnp.float32
            ).astype(jnp.bfloat16)
            rows = length * ROTARY // rank
            pieces = []
            lane = lax.broadcasted_iota(jnp.int32, (rows, 2 * ROTARY), 1)
            for pair in range(rank // (2 * ROTARY)):
                tile = block_ref[length:, pair * 2 * ROTARY : (pair + 1) * 2 * ROTARY].astype(
                    jnp.float32
                )
                other = pltpu.roll(tile, ROTARY, 1)
                pieces.append(jnp.where(lane < ROTARY, tile, other))
                pieces.append(jnp.where(lane < ROTARY, other, tile))
            turned = jnp.concatenate(pieces, axis=0).astype(jnp.bfloat16)
            key_place = block * length + lax.broadcasted_iota(jnp.int32, (length, length), 0)
            visible = key_place >= starts_ref[...]
            if own:
                query_place = me * length + lax.broadcasted_iota(jnp.int32, (length, length), 1)
                visible = visible & (key_place <= query_place)
            bias_ref[...] = jnp.where(visible, 0.0, masked_score)
            for head in range(heads):
                keys = jnp.concatenate(
                    [keys_ref[:, head * CONTENT : (head + 1) * CONTENT], turned], axis=1
                )
                scores = lax.dot_general(
                    keys,
                    query_ref[head],
                    (((1,), (1,)), ((), ())),
                    preferred_element_type=jnp.float32,
                )
                scores = scores * scale + bias_ref[...]
                highest = jnp.max(scores, axis=0, keepdims=True)
                if not own:
                    before = stat_ref[head : head + 1, :]
                    highest = jnp.maximum(highest, before)
                    factor = jnp.exp2(before - highest)
                weights = jnp.exp2(scores - highest)
                total = jnp.sum(weights, axis=0, keepdims=True)
                summed = jnp.dot(
                    values_ref[head * VALUE_DIM : (head + 1) * VALUE_DIM, :],
                    weights.astype(jnp.bfloat16),
                    preferred_element_type=jnp.float32,
                )
                if not own:
                    total = total + stat_ref[heads + head : heads + head + 1, :] * factor
                    summed = summed + acc_ref[head] * factor
                stat_ref[head : head + 1, :] = highest
                stat_ref[heads + head : heads + head + 1, :] = total
                acc_ref[head] = summed

        if own:
            work()
        else:
            needed = (block >= 0) & (block <= me) & ((block + 1) * length - 1 >= first_start)
            pl.when(needed)(work)

    for place_of, block_ref in zip(places, blocks):
        process(place_of, block_ref, place_of is own_place)


def own_place(me):
    return me


def at(flip, back):
    def place(me):
        return jnp.bitwise_xor(me, flip) - back if back else jnp.bitwise_xor(me, flip)

    return place


def finish_kernel(heads, stat_ref, acc_ref, out_ref):
    for head in range(heads):
        ratio = acc_ref[head] / stat_ref[heads + head : heads + head + 1, :]
        out_ref[:, head * VALUE_DIM : (head + 1) * VALUE_DIM] = ratio.T.astype(jnp.bfloat16)


def project_kernel(rows_ref, weight_ref, out_ref):
    out_ref[...] = jnp.dot(
        rows_ref[...], weight_ref[...], preferred_element_type=jnp.float32
    ).astype(jnp.bfloat16)


def on_device(
    query_latent,
    shared_latent,
    rotary_key,
    document_start,
    query_gain,
    shared_gain,
    content_weight,
    rotary_weight,
    key_weight,
    value_weight,
    output_weight,
):
    length, rank = shared_latent.shape
    count = lax.axis_size("sp")
    groups = lax.axis_size("tp")
    heads = key_weight.shape[1] // CONTENT
    model = output_weight.shape[1]
    me = lax.axis_index("sp")
    places = (me * length + jnp.arange(length, dtype=jnp.int32)).astype(jnp.float32)
    frequency = 1.0 / rope_theta ** (jnp.arange(0, ROTARY, 2, dtype=jnp.float32) / ROTARY)
    angles = places[:, None] * frequency[None, :]
    cosine, sine = jnp.cos(angles), jnp.sin(angles)
    cos_table = jnp.concatenate([cosine] * 4, axis=1)
    sin_table = jnp.concatenate([-sine, sine] * 2, axis=1)

    packed_rows = length + length * ROTARY // rank
    mine = pl.pallas_call(
        pack_kernel,
        out_shape=jax.ShapeDtypeStruct((packed_rows, rank), jnp.bfloat16),
        in_specs=[vmem()] * 5,
        out_specs=vmem(),
        cost_estimate=pl.CostEstimate(flops=10**8, bytes_accessed=10**6, transcendentals=0),
        compiler_params=grant(8),
        name="pack",
    )(shared_latent, rotary_key, shared_gain[None, :], cos_table, sin_table)

    everyone = range(count)

    def hop(value, pairs):
        return lax.ppermute(value, "sp", pairs)

    core = [(i, i ^ 1) for i in everyone]
    ahead = [(i, i + GROUP) for i in everyone if i + GROUP < count]
    ahead_again = [(i, j) for i, j in ahead if i % GROUP > 0]
    up = [(i, i ^ 2) for i in everyone if i % GROUP < 2]
    down = [(i, i ^ 2) for i in everyone if i % GROUP >= 2]
    both = [(i, i ^ 2) for i in everyone]

    back1 = hop(mine, ahead)
    side0 = hop(mine, up)
    core0 = hop(mine, core)
    back2 = hop(back1, ahead_again)
    side1 = hop(back1, both)
    core1 = hop(back1, core)
    far0 = hop(side0, core)
    side2 = hop(back2, down)
    core2 = hop(back2, core)
    far1 = hop(side1, core)
    far2 = hop(side2, core)

    queries = pl.pallas_call(
        query_kernel,
        out_shape=jax.ShapeDtypeStruct((heads, length, 2 * CONTENT), jnp.bfloat16),
        in_specs=[vmem()] * 6,
        out_specs=vmem(),
        cost_estimate=pl.CostEstimate(flops=8 * 10**8, bytes_accessed=4 * 10**6, transcendentals=0),
        compiler_params=grant(16),
        name="queries",
    )(query_latent, query_gain[None, :], content_weight, rotary_weight, cos_table, sin_table)

    value_turned = value_weight.T

    def attend(state, pieces):
        stage = [place for place, _ in pieces]
        arrays = [array for _, array in pieces]
        first = state is None
        operands = [document_start, document_start[None, :], queries, key_weight, value_turned]
        operands += arrays
        aliases = {}
        if not first:
            aliases = {len(operands): 0, len(operands) + 1: 1}
            operands += list(state)
        return pl.pallas_call(
            functools.partial(attend_kernel, stage, "sp", first),
            out_shape=(
                jax.ShapeDtypeStruct((2 * heads, length), jnp.float32),
                jax.ShapeDtypeStruct((heads, VALUE_DIM, length), jnp.float32),
            ),
            in_specs=[smem()] + [vmem()] * (len(operands) - 1),
            out_specs=(vmem(), vmem()),
            scratch_shapes=[
                pltpu.VMEM((length, length), jnp.float32),
                pltpu.VMEM((length, heads * CONTENT), jnp.bfloat16),
                pltpu.VMEM((heads * VALUE_DIM, length), jnp.bfloat16),
            ],
            input_output_aliases=aliases,
            cost_estimate=pl.CostEstimate(
                flops=10**9 * len(pieces), bytes_accessed=5 * 10**6, transcendentals=0
            ),
            compiler_params=grant(24),
        )(*operands)

    state = attend(None, [(own_place, mine), (at(1, 0), core0)])
    state = attend(state, [(at(2, 0), side0), (at(0, 4), back1)])
    state = attend(state, [(at(3, 0), far0), (at(1, 4), core1), (at(2, 4), side1)])
    state = attend(state, [(at(3, 4), far1), (at(1, 8), core2)])
    state = attend(state, [(at(2, 8), side2), (at(3, 8), far2)])

    attended = pl.pallas_call(
        functools.partial(finish_kernel, heads),
        out_shape=jax.ShapeDtypeStruct((length, heads * VALUE_DIM), jnp.bfloat16),
        in_specs=[vmem()] * 2,
        out_specs=vmem(),
        cost_estimate=pl.CostEstimate(flops=10**8, bytes_accessed=10**6, transcendentals=0),
        compiler_params=grant(8),
        name="finish",
    )(*state)

    chunks = 8
    width = model // chunks
    pieces = []
    for chunk in range(chunks):
        term = pl.pallas_call(
            project_kernel,
            grid=(1,),
            out_shape=jax.ShapeDtypeStruct((length, width), jnp.bfloat16),
            in_specs=[
                pl.BlockSpec((length, heads * VALUE_DIM), lambda i: (0, 0)),
                pl.BlockSpec((heads * VALUE_DIM, width), lambda i, chunk=chunk: (0, chunk)),
            ],
            out_specs=pl.BlockSpec((length, width), lambda i: (0, 0)),
            cost_estimate=pl.CostEstimate(
                flops=3 * 10**8, bytes_accessed=2 * 10**6, transcendentals=0
            ),
            compiler_params=grant(8),
        )(attended, output_weight)
        total = term.astype(jnp.float32)
        for step in range(1, groups):
            pairs = [(i, (i + step) % groups) for i in range(groups)]
            total = total + lax.ppermute(term, "tp", pairs).astype(jnp.float32)
        pieces.append(total.astype(jnp.bfloat16))
    mixed = jnp.zeros((length, model), jnp.bfloat16)
    for chunk, piece in enumerate(pieces):
        mixed = lax.dynamic_update_slice(mixed, piece, (0, chunk * width))
    return mixed


def solution(mesh):
    return jax.shard_map(
        on_device,
        mesh=mesh,
        in_specs=(
            P("sp", None),
            P("sp", None),
            P("sp", None),
            P("sp"),
            P(),
            P(),
            P(None, "tp"),
            P(None, "tp"),
            P(None, "tp"),
            P(None, "tp"),
            P("tp", None),
        ),
        out_specs=P("sp", None),
        check_vma=False,
    )
```

profile of v0, /device:TPU:12, one launch (start us, length us, event | category | flops | bytes accessed | tf_op | source)
XLA Modules:
  0.0 105.8 jit_solution(4259742446105771713)
XLA Ops:
  4.5 3.5 %collective-permute-start = (bf16[288,512]{1,0:T(8,128)(2,1)}, bf16[288,512]{1,0:T(8,128)(2,1)}, u32[]{:S(2)}, u32[]{:S(2)}) collective-permute-start(bf16[288,512]{1,0:T(8,128)(2,1)} %pack.1.refs_5_), channel_id=1, source_target_pairs={{0,8},{2,10},{4,12},{6,14},{8,16},{10,18},{12,20},{14,22},{16,24},... | collective-permute-start | bytes 884744 | tf_op jit(solution)/shard_map/ppermute | solution.py:231
  9.3 6.2 %collective-permute-done.refs_6_ = bf16[288,512]{1,0:T(8,128)(2,1)} collective-permute-done((bf16[288,512]{1,0:T(8,128)(2,1)}, bf16[288,512]{1,0:T(8,128)(2,1)}, u32[]{:S(2)}, u32[]{:S(2)}) %collective-permute-start) | collective-permute-done | bytes 294944 | tf_op jit(solution)/shard_map/ppermute | solution.py:231
  15.4 3.5 %collective-permute-start.1 = (bf16[288,512]{1,0:T(8,128)(2,1)}, bf16[288,512]{1,0:T(8,128)(2,1)}, u32[]{:S(2)}, u32[]{:S(2)}) collective-permute-start(bf16[288,512]{1,0:T(8,128)(2,1)} %collective-permute-done.refs_6_), channel_id=1, source_target_pairs={{2,10},{4,12},{6,14},{10,18},{12,20},{14,22},{18,26},{20,28},{22,3... | collective-permute-start | bytes 884744 | tf_op jit(solution)/shard_map/ppermute | solution.py:231
  19.1 1.5 %copy.23 = bf16[512,1024]{0,1:T(8,128)(2,1)S(1)} copy(bf16[512,1024]{1,0:T(8,128)(2,1)} %param.20) | data formatting | bytes 2097152 | tf_op args[9]
  22.9 1.4 %queries.1.refs_2_ = bf16[8,256,256]{2,1,0:T(8,128)(2,1)S(1)} custom-call(bf16[256,1024]{1,0:T(8,128)(2,1)S(1)} %copy-done.2, f32[1,1024]{1,0:T(1,128)S(1)} %bitcast.11, bf16[1024,1024]{1,0:T(8,128)(2,1)S(1)} %copy-done, bf16[1024,512]{1,0:T(8,128)(2,1)S(1)} %copy-done.1, f32[256,128]{1,0:T(8,128)S(1)} %get-tuple-element.28.cos_ref, ...), custom_call_target="tpu_custom_call" | custom-call | flops 800000000 | bytes 4000000 | tf_op jit(solution)/shard_map/queries/pallas_call | solution.py:252
  25.5 3.2 %collective-permute-start.2 = (bf16[288,512]{1,0:T(8,128)(2,1)}, bf16[288,512]{1,0:T(8,128)(2,1)S(1)}, u32[]{:S(2)}, u32[]{:S(2)}) collective-permute-start(bf16[288,512]{1,0:T(8,128)(2,1)} %collective-permute-done.1), channel_id=1, source_target_pairs={{4,0},{6,2},{12,8},{14,10},{20,16},{22,18},{28,24},{30,26},{5,1},{... | collective-permute-start | bytes 884744 | tf_op jit(solution)/shard_map/ppermute | solution.py:231
  28.8 3.7 %shard_map.109 = (f32[16,256]{1,0:T(8,128)S(1)}, f32[8,128,256]{2,1,0:T(8,128)S(1)}) custom-call(s32[256]{0:T(256)S(1)} %copy-done.7, s32[1,256]{1,0:T(1,128)S(1)} %bitcast.13, bf16[8,256,256]{2,1,0:T(8,128)(2,1)S(1)} %queries.1.refs_2_, bf16[512,1024]{1,0:T(8,128)(2,1)S(1)} %copy-done.6, bf16[1024,512]{1,0:T(8,128)(2,1)S(1)} %bitcast.6, ...), custom_call_target="tpu_custom_call" | custom-call | flops 2000000000 | bytes 5000000 | tf_op jit(solution)/shard_map/pallas_call | solution.py:274
  32.4 2.6 %collective-permute-start.6 = (bf16[288,512]{1,0:T(8,128)(2,1)}, bf16[288,512]{1,0:T(8,128)(2,1)S(1)}, u32[]{:S(2)}, u32[]{:S(2)}) collective-permute-start(bf16[288,512]{1,0:T(8,128)(2,1)} %collective-permute-done.1), channel_id=1, source_target_pairs={{0,2},{2,0},{4,6},{6,4},{8,10},{10,8},{12,14},{14,12},{16,18},{18,... | collective-permute-start | bytes 884744 | tf_op jit(solution)/shard_map/ppermute | solution.py:231
  35.1 6.4 %shard_map.110 = (f32[16,256]{1,0:T(8,128)S(1)}, f32[8,128,256]{2,1,0:T(8,128)S(1)}) custom-call(s32[256]{0:T(256)S(1)} %copy-done.7, s32[1,256]{1,0:T(1,128)S(1)} %bitcast.14, bf16[8,256,256]{2,1,0:T(8,128)(2,1)S(1)} %queries.1.refs_2_, bf16[512,1024]{1,0:T(8,128)(2,1)S(1)} %copy-done.6, ...), custom_call_target="tpu_custom_call", output_to_operand_aliasing={{0}: (7, {}), {1}: (8, {})} | custom-call | flops 2000000000 | bytes 5000000 | tf_op jit(solution)/shard_map/pallas_call | solution.py:274
  42.1 9.2 %shard_map.111 = (f32[16,256]{1,0:T(8,128)S(1)}, f32[8,128,256]{2,1,0:T(8,128)S(1)}) custom-call(s32[256]{0:T(256)S(1)} %copy-done.7, s32[1,256]{1,0:T(1,128)S(1)} %bitcast.15, bf16[8,256,256]{2,1,0:T(8,128)(2,1)S(1)} %queries.1.refs_2_, bf16[512,1024]{1,0:T(8,128)(2,1)S(1)} %copy-done.6, ...), custom_call_target="tpu_custom_call", output_to_operand_aliasing={{0}: (8, {}), {1}: (9, {})} | custom-call | flops 3000000000 | bytes 5000000 | tf_op jit(solution)/shard_map/pallas_call | solution.py:274
  51.3 3.3 %shard_map.112 = (f32[16,256]{1,0:T(8,128)S(1)}, f32[8,128,256]{2,1,0:T(8,128)S(1)}) custom-call(s32[256]{0:T(256)S(1)} %copy-done.7, s32[1,256]{1,0:T(1,128)S(1)} %bitcast.16, bf16[8,256,256]{2,1,0:T(8,128)(2,1)S(1)} %queries.1.refs_2_, bf16[512,1024]{1,0:T(8,128)(2,1)S(1)} %copy-done.6, ...), custom_call_target="tpu_custom_call", output_to_operand_aliasing={{0}: (7, {}), {1}: (8, {})} | custom-call | flops 2000000000 | bytes 5000000 | tf_op jit(solution)/shard_map/pallas_call | solution.py:274
  57.3 1.5 %collective-permute-start.11 = (bf16[256,512]{1,0:T(8,128)(2,1)S(1)}, bf16[256,512]{1,0:T(8,128)(2,1)S(1)}, u32[]{:S(2)}, u32[]{:S(2)}) collective-permute-start(bf16[256,512]{1,0:T(8,128)(2,1)S(1)} %shard_map.114), channel_id=1, source_target_pairs={{0,1},{1,0},{2,3},{3,2},{4,5},{5,4},{6,7},{7,6},{8,9},{9,8},{10,11... | collective-permute-start | bytes 786440 | tf_op jit(solution)/shard_map/ppermute | solution.py:331
  60.4 1.5 %collective-permute-start.13 = (bf16[256,512]{1,0:T(8,128)(2,1)S(1)}, bf16[256,512]{1,0:T(8,128)(2,1)S(1)}, u32[]{:S(2)}, u32[]{:S(2)}) collective-permute-start(bf16[256,512]{1,0:T(8,128)(2,1)S(1)} %shard_map.116), channel_id=1, source_target_pairs={{0,1},{1,0},{2,3},{3,2},{4,5},{5,4},{6,7},{7,6},{8,9},{9,8},{10,11... | collective-permute-start | bytes 786440 | tf_op jit(solution)/shard_map/ppermute | solution.py:331
  63.4 1.5 %collective-permute-start.15 = (bf16[256,512]{1,0:T(8,128)(2,1)S(1)}, bf16[256,512]{1,0:T(8,128)(2,1)S(1)}, u32[]{:S(2)}, u32[]{:S(2)}) collective-permute-start(bf16[256,512]{1,0:T(8,128)(2,1)S(1)} %shard_map.118), channel_id=1, source_target_pairs={{0,1},{1,0},{2,3},{3,2},{4,5},{5,4},{6,7},{7,6},{8,9},{9,8},{10,11... | collective-permute-start | bytes 786440 | tf_op jit(solution)/shard_map/ppermute | solution.py:331
  66.6 1.5 %collective-permute-start.16 = (bf16[256,512]{1,0:T(8,128)(2,1)S(1)}, bf16[256,512]{1,0:T(8,128)(2,1)S(1)}, u32[]{:S(2)}, u32[]{:S(2)}) collective-permute-start(bf16[256,512]{1,0:T(8,128)(2,1)S(1)} %shard_map.119), channel_id=1, source_target_pairs={{0,1},{1,0},{2,3},{3,2},{4,5},{5,4},{6,7},{7,6},{8,9},{9,8},{10,11... | collective-permute-start | bytes 786440 | tf_op jit(solution)/shard_map/ppermute | solution.py:331
  68.4 3.8 %collective-permute-done.12 = bf16[256,512]{1,0:T(8,128)(2,1)S(1)} collective-permute-done((bf16[256,512]{1,0:T(8,128)(2,1)S(1)}, bf16[256,512]{1,0:T(8,128)(2,1)S(1)}, u32[]{:S(2)}, u32[]{:S(2)}) %collective-permute-start.12) | collective-permute-done | bytes 262176 | tf_op jit(solution)/shard_map/ppermute | solution.py:331
  72.2 1.5 %collective-permute-start.17 = (bf16[256,512]{1,0:T(8,128)(2,1)S(1)}, bf16[256,512]{1,0:T(8,128)(2,1)S(1)}, u32[]{:S(2)}, u32[]{:S(2)}) collective-permute-start(bf16[256,512]{1,0:T(8,128)(2,1)S(1)} %shard_map.120), channel_id=1, source_target_pairs={{0,1},{1,0},{2,3},{3,2},{4,5},{5,4},{6,7},{7,6},{8,9},{9,8},{10,11... | collective-permute-start | bytes 786440 | tf_op jit(solution)/shard_map/ppermute | solution.py:331
  73.7 4.1 %collective-permute-done.13 = bf16[256,512]{1,0:T(8,128)(2,1)S(1)} collective-permute-done((bf16[256,512]{1,0:T(8,128)(2,1)S(1)}, bf16[256,512]{1,0:T(8,128)(2,1)S(1)}, u32[]{:S(2)}, u32[]{:S(2)}) %collective-permute-start.13) | collective-permute-done | bytes 262176 | tf_op jit(solution)/shard_map/ppermute | solution.py:331
  77.8 1.5 %collective-permute-start.18 = (bf16[256,512]{1,0:T(8,128)(2,1)S(1)}, bf16[256,512]{1,0:T(8,128)(2,1)S(1)}, u32[]{:S(2)}, u32[]{:S(2)}) collective-permute-start(bf16[256,512]{1,0:T(8,128)(2,1)S(1)} %shard_map.121), channel_id=1, source_target_pairs={{0,1},{1,0},{2,3},{3,2},{4,5},{5,4},{6,7},{7,6},{8,9},{9,8},{10,11... | collective-permute-start | bytes 786440 | tf_op jit(solution)/shard_map/ppermute | solution.py:331
  79.4 4.1 %collective-permute-done.14 = bf16[256,512]{1,0:T(8,128)(2,1)S(1)} collective-permute-done((bf16[256,512]{1,0:T(8,128)(2,1)S(1)}, bf16[256,512]{1,0:T(8,128)(2,1)S(1)}, u32[]{:S(2)}, u32[]{:S(2)}) %collective-permute-start.14) | collective-permute-done | bytes 262176 | tf_op jit(solution)/shard_map/ppermute | solution.py:331
  83.5 5.5 %collective-permute-done.15 = bf16[256,512]{1,0:T(8,128)(2,1)S(1)} collective-permute-done((bf16[256,512]{1,0:T(8,128)(2,1)S(1)}, bf16[256,512]{1,0:T(8,128)(2,1)S(1)}, u32[]{:S(2)}, u32[]{:S(2)}) %collective-permute-start.15) | collective-permute-done | bytes 262176 | tf_op jit(solution)/shard_map/ppermute | solution.py:331
  89.1 5.5 %collective-permute-done.16 = bf16[256,512]{1,0:T(8,128)(2,1)S(1)} collective-permute-done((bf16[256,512]{1,0:T(8,128)(2,1)S(1)}, bf16[256,512]{1,0:T(8,128)(2,1)S(1)}, u32[]{:S(2)}, u32[]{:S(2)}) %collective-permute-start.16) | collective-permute-done | bytes 262176 | tf_op jit(solution)/shard_map/ppermute | solution.py:331
  94.7 5.5 %collective-permute-done.17 = bf16[256,512]{1,0:T(8,128)(2,1)S(1)} collective-permute-done((bf16[256,512]{1,0:T(8,128)(2,1)S(1)}, bf16[256,512]{1,0:T(8,128)(2,1)S(1)}, u32[]{:S(2)}, u32[]{:S(2)}) %collective-permute-start.17) | collective-permute-done | bytes 262176 | tf_op jit(solution)/shard_map/ppermute | solution.py:331
  100.4 4.7 %collective-permute-done.18 = bf16[256,512]{1,0:T(8,128)(2,1)S(1)} collective-permute-done((bf16[256,512]{1,0:T(8,128)(2,1)S(1)}, bf16[256,512]{1,0:T(8,128)(2,1)S(1)}, u32[]{:S(2)}, u32[]{:S(2)}) %collective-permute-start.18) | collective-permute-done | bytes 262176 | tf_op jit(solution)/shard_map/ppermute | solution.py:331
  (68 shorter events, 18.7 us)
Async XLA Ops:
  0.0 20.6 %copy-start = (bf16[1024,1024]{1,0:T(8,128)(2,1)S(1)}, bf16[1024,1024]{1,0:T(8,128)(2,1)}, u32[]{:S(2)}) copy-start(bf16[1024,1024]{1,0:T(8,128)(2,1)} %content_ref.1) | copy-start | bytes 6291460
  3.5 17.1 %copy-start.4 = (f32[1024]{0:T(1024)S(1)}, f32[1024]{0:T(1024)}, u32[]{:S(2)}) copy-start(f32[1024]{0:T(1024)} %param.15) | copy-start | bytes 12292
  4.5 10.9 %collective-permute-start = (bf16[288,512]{1,0:T(8,128)(2,1)}, bf16[288,512]{1,0:T(8,128)(2,1)}, u32[]{:S(2)}, u32[]{:S(2)}) collective-permute-start(bf16[288,512]{1,0:T(8,128)(2,1)} %pack.1.refs_5_), channel_id=1, source_target_pairs={{0,8},{2,10},{4,12},{6,14},{8,16},{10,18},{12,20},{14,22},{16,24},... | collective-permute-start | bytes 884744 | tf_op jit(solution)/shard_map/ppermute | solution.py:231
  8.0 16.8 %collective-permute-start.7 = (bf16[288,512]{1,0:T(8,128)(2,1)}, bf16[288,512]{1,0:T(8,128)(2,1)}, u32[]{:S(2)}, u32[]{:S(2)}) collective-permute-start(bf16[288,512]{1,0:T(8,128)(2,1)} %pack.1.refs_5_), channel_id=1, source_target_pairs={{0,4},{2,6},{8,12},{10,14},{16,20},{18,22},{24,28},{26,30},{1,5},{... | collective-permute-start | bytes 884744 | tf_op jit(solution)/shard_map/ppermute | solution.py:231
  15.4 10.1 %collective-permute-start.1 = (bf16[288,512]{1,0:T(8,128)(2,1)}, bf16[288,512]{1,0:T(8,128)(2,1)}, u32[]{:S(2)}, u32[]{:S(2)}) collective-permute-start(bf16[288,512]{1,0:T(8,128)(2,1)} %collective-permute-done.refs_6_), channel_id=1, source_target_pairs={{2,10},{4,12},{6,14},{10,18},{12,20},{14,22},{18,26},{20,28},{22,3... | collective-permute-start | bytes 884744 | tf_op jit(solution)/shard_map/ppermute | solution.py:231
  18.9 9.8 %collective-permute-start.10 = (bf16[288,512]{1,0:T(8,128)(2,1)}, bf16[288,512]{1,0:T(8,128)(2,1)}, u32[]{:S(2)}, u32[]{:S(2)}) collective-permute-start(bf16[288,512]{1,0:T(8,128)(2,1)} %pack.1.refs_5_), channel_id=1, source_target_pairs={{0,2},{2,0},{4,6},{6,4},{8,10},{10,8},{12,14},{14,12},{16,18},{18,... | collective-permute-start | bytes 884744 | tf_op jit(solution)/shard_map/ppermute | solution.py:231
  19.0 16.0 %collective-permute-start.4 = (bf16[288,512]{1,0:T(8,128)(2,1)}, bf16[288,512]{1,0:T(8,128)(2,1)}, u32[]{:S(2)}, u32[]{:S(2)}) collective-permute-start(bf16[288,512]{1,0:T(8,128)(2,1)} %collective-permute-done.refs_6_), channel_id=1, source_target_pairs={{0,4},{2,6},{4,0},{6,2},{8,12},{10,14},{12,8},{14,10},{16,20},{18,... | collective-permute-start | bytes 884744 | tf_op jit(solution)/shard_map/ppermute | solution.py:231
  22.9 5.9 %copy-start.6 = (bf16[512,1024]{1,0:T(8,128)(2,1)S(1)}, bf16[512,1024]{1,0:T(8,128)(2,1)}, u32[]{:S(2)}) copy-start(bf16[512,1024]{1,0:T(8,128)(2,1)} %refs_3_.9) | copy-start | bytes 3145732
  22.9 5.9 %copy-start.7 = (s32[256]{0:T(256)S(1)}, s32[256]{0:T(256)}, u32[]{:S(2)}) copy-start(s32[256]{0:T(256)} %refs_0_.9) | copy-start | bytes 3076
  24.2 17.8 %collective-permute-start.9 = (bf16[288,512]{1,0:T(8,128)(2,1)}, bf16[288,512]{1,0:T(8,128)(2,1)S(1)}, u32[]{:S(2)}, u32[]{:S(2)}) collective-permute-start(bf16[288,512]{1,0:T(8,128)(2,1)} %collective-permute-done.refs_6_), channel_id=1, source_target_pairs={{0,2},{2,0},{4,6},{6,4},{8,10},{10,8},{12,14},{14,12},{16,18},{18,... | collective-permute-start | bytes 884744 | tf_op jit(solution)/shard_map/ppermute | solution.py:231
  24.7 17.4 %collective-permute-start.8 = (bf16[288,512]{1,0:T(8,128)(2,1)}, bf16[288,512]{1,0:T(8,128)(2,1)S(1)}, u32[]{:S(2)}, u32[]{:S(2)}) collective-permute-start(bf16[288,512]{1,0:T(8,128)(2,1)} %collective-permute-done.7.refs_5_), channel_id=1, source_target_pairs={{0,2},{2,0},{4,6},{6,4},{8,10},{10,8},{12,14},{14,12},{16,18},{18,... | collective-permute-start | bytes 884744 | tf_op jit(solution)/shard_map/ppermute | solution.py:231
  25.5 16.1 %collective-permute-start.2 = (bf16[288,512]{1,0:T(8,128)(2,1)}, bf16[288,512]{1,0:T(8,128)(2,1)S(1)}, u32[]{:S(2)}, u32[]{:S(2)}) collective-permute-start(bf16[288,512]{1,0:T(8,128)(2,1)} %collective-permute-done.1), channel_id=1, source_target_pairs={{4,0},{6,2},{12,8},{14,10},{20,16},{22,18},{28,24},{30,26},{5,1},{... | collective-permute-start | bytes 884744 | tf_op jit(solution)/shard_map/ppermute | solution.py:231
  32.4 18.9 %collective-permute-start.6 = (bf16[288,512]{1,0:T(8,128)(2,1)}, bf16[288,512]{1,0:T(8,128)(2,1)S(1)}, u32[]{:S(2)}, u32[]{:S(2)}) collective-permute-start(bf16[288,512]{1,0:T(8,128)(2,1)} %collective-permute-done.1), channel_id=1, source_target_pairs={{0,2},{2,0},{4,6},{6,4},{8,10},{10,8},{12,14},{14,12},{16,18},{18,... | collective-permute-start | bytes 884744 | tf_op jit(solution)/shard_map/ppermute | solution.py:231
  35.0 16.3 %collective-permute-start.5 = (bf16[288,512]{1,0:T(8,128)(2,1)}, bf16[288,512]{1,0:T(8,128)(2,1)S(1)}, u32[]{:S(2)}, u32[]{:S(2)}) collective-permute-start(bf16[288,512]{1,0:T(8,128)(2,1)} %collective-permute-done.4.refs_7_), channel_id=1, source_target_pairs={{0,2},{2,0},{4,6},{6,4},{8,10},{10,8},{12,14},{14,12},{16,18},{18,... | collective-permute-start | bytes 884744 | tf_op jit(solution)/shard_map/ppermute | solution.py:231
  41.6 13.1 %collective-permute-start.3 = (bf16[288,512]{1,0:T(8,128)(2,1)S(1)}, bf16[288,512]{1,0:T(8,128)(2,1)S(1)}, u32[]{:S(2)}, u32[]{:S(2)}) collective-permute-start(bf16[288,512]{1,0:T(8,128)(2,1)S(1)} %collective-permute-done.2.refs_5_), channel_id=1, source_target_pairs={{0,2},{2,0},{4,6},{6,4},{8,10},{10,8},{12,14},{14,12},{16,18},{18,... | collective-permute-start | bytes 884744 | tf_op jit(solution)/shard_map/ppermute | solution.py:231
  57.3 9.2 %collective-permute-start.11 = (bf16[256,512]{1,0:T(8,128)(2,1)S(1)}, bf16[256,512]{1,0:T(8,128)(2,1)S(1)}, u32[]{:S(2)}, u32[]{:S(2)}) collective-permute-start(bf16[256,512]{1,0:T(8,128)(2,1)S(1)} %shard_map.114), channel_id=1, source_target_pairs={{0,1},{1,0},{2,3},{3,2},{4,5},{5,4},{6,7},{7,6},{8,9},{9,8},{10,11... | collective-permute-start | bytes 786440 | tf_op jit(solution)/shard_map/ppermute | solution.py:331
  59.3 12.9 %collective-permute-start.12 = (bf16[256,512]{1,0:T(8,128)(2,1)S(1)}, bf16[256,512]{1,0:T(8,128)(2,1)S(1)}, u32[]{:S(2)}, u32[]{:S(2)}) collective-permute-start(bf16[256,512]{1,0:T(8,128)(2,1)S(1)} %shard_map.115), channel_id=1, source_target_pairs={{0,1},{1,0},{2,3},{3,2},{4,5},{5,4},{6,7},{7,6},{8,9},{9,8},{10,11... | collective-permute-start | bytes 786440 | tf_op jit(solution)/shard_map/ppermute | solution.py:331
  60.4 17.4 %collective-permute-start.13 = (bf16[256,512]{1,0:T(8,128)(2,1)S(1)}, bf16[256,512]{1,0:T(8,128)(2,1)S(1)}, u32[]{:S(2)}, u32[]{:S(2)}) collective-permute-start(bf16[256,512]{1,0:T(8,128)(2,1)S(1)} %shard_map.116), channel_id=1, source_target_pairs={{0,1},{1,0},{2,3},{3,2},{4,5},{5,4},{6,7},{7,6},{8,9},{9,8},{10,11... | collective-permute-start | bytes 786440 | tf_op jit(solution)/shard_map/ppermute | solution.py:331
  62.4 21.1 %collective-permute-start.14 = (bf16[256,512]{1,0:T(8,128)(2,1)S(1)}, bf16[256,512]{1,0:T(8,128)(2,1)S(1)}, u32[]{:S(2)}, u32[]{:S(2)}) collective-permute-start(bf16[256,512]{1,0:T(8,128)(2,1)S(1)} %shard_map.117), channel_id=1, source_target_pairs={{0,1},{1,0},{2,3},{3,2},{4,5},{5,4},{6,7},{7,6},{8,9},{9,8},{10,11... | collective-permute-start | bytes 786440 | tf_op jit(solution)/shard_map/ppermute | solution.py:331
  63.4 25.6 %collective-permute-start.15 = (bf16[256,512]{1,0:T(8,128)(2,1)S(1)}, bf16[256,512]{1,0:T(8,128)(2,1)S(1)}, u32[]{:S(2)}, u32[]{:S(2)}) collective-permute-start(bf16[256,512]{1,0:T(8,128)(2,1)S(1)} %shard_map.118), channel_id=1, source_target_pairs={{0,1},{1,0},{2,3},{3,2},{4,5},{5,4},{6,7},{7,6},{8,9},{9,8},{10,11... | collective-permute-start | bytes 786440 | tf_op jit(solution)/shard_map/ppermute | solution.py:331
  66.6 28.1 %collective-permute-start.16 = (bf16[256,512]{1,0:T(8,128)(2,1)S(1)}, bf16[256,512]{1,0:T(8,128)(2,1)S(1)}, u32[]{:S(2)}, u32[]{:S(2)}) collective-permute-start(bf16[256,512]{1,0:T(8,128)(2,1)S(1)} %shard_map.119), channel_id=1, source_target_pairs={{0,1},{1,0},{2,3},{3,2},{4,5},{5,4},{6,7},{7,6},{8,9},{9,8},{10,11... | collective-permute-start | bytes 786440 | tf_op jit(solution)/shard_map/ppermute | solution.py:331
  72.2 28.1 %collective-permute-start.17 = (bf16[256,512]{1,0:T(8,128)(2,1)S(1)}, bf16[256,512]{1,0:T(8,128)(2,1)S(1)}, u32[]{:S(2)}, u32[]{:S(2)}) collective-permute-start(bf16[256,512]{1,0:T(8,128)(2,1)S(1)} %shard_map.120), channel_id=1, source_target_pairs={{0,1},{1,0},{2,3},{3,2},{4,5},{5,4},{6,7},{7,6},{8,9},{9,8},{10,11... | collective-permute-start | bytes 786440 | tf_op jit(solution)/shard_map/ppermute | solution.py:331
  77.8 27.2 %collective-permute-start.18 = (bf16[256,512]{1,0:T(8,128)(2,1)S(1)}, bf16[256,512]{1,0:T(8,128)(2,1)S(1)}, u32[]{:S(2)}, u32[]{:S(2)}) collective-permute-start(bf16[256,512]{1,0:T(8,128)(2,1)S(1)} %shard_map.121), channel_id=1, source_target_pairs={{0,1},{1,0},{2,3},{3,2},{4,5},{5,4},{6,7},{7,6},{8,9},{9,8},{10,11... | collective-permute-start | bytes 786440 | tf_op jit(solution)/shard_map/ppermute | solution.py:331
  100.4 4.7 %copy-start.8 = (bf16[256,4096]{1,0:T(8,128)(2,1)}, bf16[256,4096]{1,0:T(8,128)(2,1)S(1)}, u32[]{:S(2)}) copy-start(bf16[256,4096]{1,0:T(8,128)(2,1)S(1)} %fusion.5) | copy-start | bytes 6291460
  (6 other events, 10.6 us)
where the time goes:
time: 106 us
  waiting for transfers between devices  40.4 us (38%)
  Pallas kernels  29.6 us (28%)
  starting transfers between devices  25.6 us (24%)
  local copies, waits for them, and re-layouts  7.68 us (7%)
  other arithmetic  2.07 us (2%)
    ppermute x8, waiting for transfers between devices, on_device(): total = total + lax.ppermute(term, 'tp', pairs).astype(jnp.float32)  33.5 us
    pallas_call x5, Pallas kernels, attend(): pl.pallas_call(functools.partial(attend_kernel, stage, 'sp', first), out_...  23.6 us
    ppermute x11, starting transfers between devices, hop(): return lax.ppermute(value, 'sp', pairs)  15.4 us
    ppermute x8, starting transfers between devices, on_device(): total = total + lax.ppermute(term, 'tp', pairs).astype(jnp.float32)  10.3 us
    unnamed x24, local copies, waits for them, and re-layouts  7.45 us
    ppermute x11, waiting for transfers between devices, hop(): return lax.ppermute(value, 'sp', pairs)  6.88 us
    pallas_call x8, Pallas kernels, on_device(): pl.pallas_call(project_kernel, grid=(1,), out_shape=jax.ShapeDtypeStruct(...  3.51 us
  transfers between devices with their start and end apart: 19, of which 10 were waited for; matrix products, arithmetic and copies ran while one was open for 2% of the time, Pallas kernels for 26%

commit v1 on v0

v1 whole, which is shorter than its diff:
```python
import functools

import jax
import jax.numpy as jnp
from jax import lax
from jax.experimental import pallas as pl
from jax.experimental.pallas import tpu as pltpu
from jax.sharding import PartitionSpec as P

CONTENT = 128
ROTARY = 64
VALUE_DIM = 128
GROUP = 4
KINDS = ("quad", "pair", "pair")

norm_eps = 1e-06
rope_theta = 10000.0
masked_score = -1e30
LOG2E = 1.4426950408889634


def vmem():
    return pl.BlockSpec(memory_space=pltpu.VMEM)


def grant(mebibytes):
    return pltpu.CompilerParams(vmem_limit_bytes=mebibytes * 2**20)


def hbm():
    return pl.BlockSpec(memory_space=pltpu.HBM)


def smem():
    return pl.BlockSpec(memory_space=pltpu.SMEM)


def normed(latent, gain):
    entries = latent.astype(jnp.float32)
    scale = lax.rsqrt(jnp.mean(entries * entries, axis=-1, keepdims=True) + norm_eps)
    return (entries * scale * gain).astype(jnp.bfloat16)


def swap_halves(x):
    width = x.shape[-1]
    half = ROTARY // 2
    lane = lax.broadcasted_iota(jnp.int32, x.shape, x.ndim - 1)
    ahead = pltpu.roll(x, width - half, x.ndim - 1)
    behind = pltpu.roll(x, half, x.ndim - 1)
    return jnp.where(lane % ROTARY < half, ahead, behind)


def load(pairs, sems):
    copies = [pltpu.make_async_copy(src, dst, sems.at[k]) for k, (src, dst) in enumerate(pairs)]
    for copy in copies:
        copy.start()
    return copies


def pack_kernel(cuts, axis, shared_hbm, rotary_hbm, gain_hbm, weight_hbm, cos_ref, sin_ref, *refs):
    out_ref, parts, refs = refs[0], refs[1 : 1 + len(cuts)], refs[1 + len(cuts) :]
    shared_ref, rotary_ref, gain_ref, sems = refs
    length, rank = shared_ref.shape
    half = ROTARY // 2
    me = lax.axis_index(axis)
    pairs = [(rotary_hbm, rotary_ref), (gain_hbm, gain_ref), (shared_hbm, shared_ref)]
    for (base, size, kind), part_ref in zip(cuts, parts):
        start = pl.multiple_of(base + slot_of(me, kind) * size, 128)
        pairs.append((weight_hbm.at[:, pl.ds(start, size)], part_ref))
    copies = load(pairs, sems)
    copies[0].wait()
    key = rotary_ref[...].astype(jnp.float32)
    low, high = key[:half], key[half:]
    cosine, sine = cos_ref[...], sin_ref[...]
    turned = jnp.concatenate([low * cosine - high * sine, low * sine + high * cosine], axis=0)
    turned = jnp.concatenate([turned, turned], axis=0).T
    rows = length * ROTARY // rank
    lane = lax.broadcasted_iota(jnp.int32, (rows, 2 * ROTARY), 1)
    for pair in range(rank // (2 * ROTARY)):
        low = turned[(2 * pair) * rows : (2 * pair + 1) * rows]
        high = turned[(2 * pair + 1) * rows : (2 * pair + 2) * rows]
        out_ref[length:, pair * 2 * ROTARY : (pair + 1) * 2 * ROTARY] = jnp.where(
            lane < ROTARY, low, high
        ).astype(jnp.bfloat16)
    copies[1].wait()
    copies[2].wait()
    out_ref[0:length, :] = normed(shared_ref[...], gain_ref[...])
    for copy in copies[3:]:
        copy.wait()


def begin_kernel(axis, *refs):
    hbm, refs = refs[:6], refs[6:]
    starts_ref, block_ref, cos_ref, sin_ref = refs[:4]
    query_ref, turned_value_ref, stat_ref, acc_ref = refs[4:8]
    held, refs = refs[8:14], refs[14:]
    scratch, sems = refs[:-1], refs[-1]
    copies = load(list(zip(hbm, held)), sems)
    latent_ref, gain_ref, content_ref, rotary_ref, value_ref, key_ref = held
    cos4 = jnp.concatenate([cos_ref[...]] * 4, axis=0).T
    sin4 = jnp.concatenate([-sin_ref[...], sin_ref[...]] * 2, axis=0).T
    copies[0].wait()
    copies[1].wait()
    rows = normed(latent_ref[...], gain_ref[...])
    copies[2].wait()
    content = jnp.dot(rows, content_ref[...], preferred_element_type=jnp.float32)
    for head in range(query_ref.shape[0]):
        query_ref[head, :, 0:CONTENT] = content[:, head * CONTENT : (head + 1) * CONTENT].astype(
            jnp.bfloat16
        )
    copies[3].wait()
    raw = jnp.dot(rows, rotary_ref[...], preferred_element_type=jnp.float32)
    lane = lax.broadcasted_iota(jnp.int32, (rows.shape[0], 2 * ROTARY), 1)
    for pair in range(query_ref.shape[0] // 2):
        piece = raw[:, pair * 2 * ROTARY : (pair + 1) * 2 * ROTARY]
        turned = piece * cos4 + swap_halves(piece) * sin4
        for side in range(2):
            own = (lane < ROTARY) if side == 0 else (lane >= ROTARY)
            query_ref[2 * pair + side, :, CONTENT:] = jnp.where(own, turned, 0.0).astype(
                jnp.bfloat16
            )
    copies[4].wait()
    turned_value_ref[...] = value_ref[...].T
    copies[5].wait()
    me = lax.axis_index(axis)
    absorb(
        me, me, True, block_ref, starts_ref, query_ref, key_ref, turned_value_ref, stat_ref, acc_ref, *scratch
    )


def absorb(
    me, block, own, block_ref, starts_ref, query_ref, key_ref, value_ref, stat_ref, acc_ref,
    bias_ref, keys_ref, values_ref, scores_ref, weights_ref,
):
    heads, length = query_ref.shape[0], query_ref.shape[1]
    rank = key_ref.shape[0]
    scale = (CONTENT + ROTARY) ** (-0.5) * LOG2E
    shared = block_ref[0:length, :]
    keys_ref[...] = jnp.dot(shared, key_ref[...], preferred_element_type=jnp.float32).astype(
        jnp.bfloat16
    )
    values_ref[...] = lax.dot_general(
        value_ref[...], shared, (((1,), (1,)), ((), ())), preferred_element_type=jnp.float32
    ).astype(jnp.bfloat16)
    rows = length * ROTARY // rank
    pieces = []
    lane = lax.broadcasted_iota(jnp.int32, (rows, 2 * ROTARY), 1)
    for pair in range(rank // (2 * ROTARY)):
        tile = block_ref[length:, pair * 2 * ROTARY : (pair + 1) * 2 * ROTARY].astype(jnp.float32)
        other = pltpu.roll(tile, ROTARY, 1)
        pieces.append(jnp.where(lane < ROTARY, tile, other))
        pieces.append(jnp.where(lane < ROTARY, other, tile))
    turned = jnp.concatenate(pieces, axis=0).astype(jnp.bfloat16)
    key_place = block * length + lax.broadcasted_iota(jnp.int32, (length, length), 0)
    visible = key_place >= starts_ref[...]
    if own:
        query_place = me * length + lax.broadcasted_iota(jnp.int32, (length, length), 1)
        visible = visible & (key_place <= query_place)
    bias_ref[...] = jnp.where(visible, 0.0, masked_score)
    tops, factors = [], []
    for head in range(heads):
        keys = jnp.concatenate([keys_ref[:, head * CONTENT : (head + 1) * CONTENT], turned], axis=1)
        scores = lax.dot_general(
            keys, query_ref[head], (((1,), (1,)), ((), ())), preferred_element_type=jnp.float32
        )
        scores = scores * scale + bias_ref[...]
        scores_ref[head] = scores
        highest = jnp.max(scores, axis=0, keepdims=True)
        if not own:
            highest = jnp.maximum(highest, stat_ref[head : head + 1, :])
        tops.append(highest)
    piece = 64
    for head in range(heads):
        total = jnp.zeros((1, length), jnp.float32)
        for row in range(0, length, piece):
            weights = jnp.exp2(scores_ref[head, row : row + piece, :] - tops[head])
            total = total + jnp.sum(weights, axis=0, keepdims=True)
            weights_ref[head, row : row + piece, :] = weights.astype(jnp.bfloat16)
        if not own:
            factor = jnp.exp2(stat_ref[head : head + 1, :] - tops[head])
            factors.append(factor)
            total = total + stat_ref[heads + head : heads + head + 1, :] * factor
        stat_ref[head : head + 1, :] = tops[head]
        stat_ref[heads + head : heads + head + 1, :] = total
    for head in range(heads):
        summed = jnp.dot(
            values_ref[head * VALUE_DIM : (head + 1) * VALUE_DIM, :],
            weights_ref[head],
            preferred_element_type=jnp.float32,
        )
        acc_ref[head] = summed if own else acc_ref[head] * factors[head] + summed


def work_area(heads, length):
    return [
        pltpu.VMEM((length, length), jnp.float32),
        pltpu.VMEM((length, heads * CONTENT), jnp.bfloat16),
        pltpu.VMEM((heads * VALUE_DIM, length), jnp.bfloat16),
        pltpu.VMEM((heads, length, length), jnp.float32),
        pltpu.VMEM((heads, length, length), jnp.bfloat16),
    ]


def attend_kernel(places, axis, *refs):
    count = len(places)
    starts_smem, starts_ref, query_ref, key_ref, value_ref = refs[:5]
    blocks, refs = refs[5 : 5 + count], refs[5 + count :]
    old_stat, old_acc, stat_ref, acc_ref = refs[:4]
    scratch = refs[4:]
    length = query_ref.shape[1]
    me = lax.axis_index(axis)
    stat_ref[...] = old_stat[...]
    acc_ref[...] = old_acc[...]
    for place_of, block_ref in zip(places, blocks):
        block = place_of(me)
        needed = (block >= 0) & (block <= me) & ((block + 1) * length - 1 >= starts_smem[0])
        pl.when(needed)(
            functools.partial(
                absorb, me, block, False, block_ref, starts_ref, query_ref, key_ref, value_ref,
                stat_ref, acc_ref, *scratch,
            )
        )


def at(flip, back):
    def place(me):
        return jnp.bitwise_xor(me, flip) - back if back else jnp.bitwise_xor(me, flip)

    return place


def finish_kernel(heads, stat_ref, acc_ref, out_ref):
    for head in range(heads):
        ratio = acc_ref[head] / stat_ref[heads + head : heads + head + 1, :]
        out_ref[:, head * VALUE_DIM : (head + 1) * VALUE_DIM] = ratio.T.astype(jnp.bfloat16)


def project_kernel(rows_ref, weight_ref, out_ref):
    tile = 512

    @pl.loop(0, weight_ref.shape[1] // tile)
    def _(step):
        columns = pl.ds(pl.multiple_of(step * tile, tile), tile)
        out_ref[:, columns] = jnp.dot(
            rows_ref[...], weight_ref[:, columns], preferred_element_type=jnp.float32
        ).astype(jnp.bfloat16)


def slot_of(me, kind):
    if kind == "quad":
        return jnp.bitwise_and(me, 7)
    return jnp.bitwise_and(lax.shift_right_logical(me, 2), 1) * 2 + jnp.bitwise_and(me, 1)


def combine_kernel(places, axis, rows_ref, ours_ref, *refs):
    me = lax.axis_index(axis)
    count = len(places)
    pieces, out_hbm, refs = refs[:count], refs[count], refs[count + 1 :]
    held_ref, done_ref, sems, out_sems = refs
    copies = []
    for k, (base, size, kind, change) in enumerate(places):
        start = base + jnp.bitwise_xor(slot_of(me, kind), change) * size
        columns = pl.ds(pl.multiple_of(start, 128), size)
        copies.append(pltpu.make_async_copy(pieces[k], held_ref.at[:, columns], sems.at[k]))
    ahead = 6
    for copy in copies[:ahead]:
        copy.start()
    leaving = []
    for k in range(0, count, 2):
        base, size, kind, change = places[k]
        start = base + (jnp.bitwise_xor(slot_of(me, kind), change) // 2) * (2 * size)
        columns = pl.ds(pl.multiple_of(start, 256), 2 * size)
        for late in (k, k + 1):
            copies[late].wait()
            if late + ahead < count:
                copies[late + ahead].start()
        term = jnp.dot(rows_ref[...], held_ref[:, columns], preferred_element_type=jnp.float32)
        term = term.astype(jnp.bfloat16).astype(jnp.float32)
        done_ref[:, columns] = (ours_ref[:, columns].astype(jnp.float32) + term).astype(
            jnp.bfloat16
        )
        out = pltpu.make_async_copy(
            done_ref.at[:, columns], out_hbm.at[:, columns], out_sems.at[k // 2]
        )
        out.start()
        leaving.append(out)
    for out in leaving:
        out.wait()


def on_device(
    query_latent,
    shared_latent,
    rotary_key,
    document_start,
    query_gain,
    shared_gain,
    content_weight,
    rotary_weight,
    key_weight,
    value_weight,
    output_weight,
):
    length, rank = shared_latent.shape
    count = lax.axis_size("sp")
    groups = lax.axis_size("tp")
    heads = key_weight.shape[1] // CONTENT
    model = output_weight.shape[1]
    me = lax.axis_index("sp")
    position = (me * length + jnp.arange(length, dtype=jnp.int32)).astype(jnp.float32)
    frequency = 1.0 / rope_theta ** (jnp.arange(0, ROTARY, 2, dtype=jnp.float32) / ROTARY)
    angles = frequency[:, None] * position[None, :]
    cosine, sine = jnp.cos(angles), jnp.sin(angles)

    plan = groups == 2 and count % 8 == 0 and model % 2048 == 0
    swap = [(0, 1), (1, 0)]
    size = model // 16
    cuts, base = [], 0
    for kind in KINDS if plan else ():
        cuts.append((base, size, kind))
        base += size * (8 if kind == "quad" else 4)

    packed_rows = length + length * ROTARY // rank
    mine, *parts = pl.pallas_call(
        functools.partial(pack_kernel, cuts, "sp"),
        out_shape=[jax.ShapeDtypeStruct((packed_rows, rank), jnp.bfloat16)]
        + [jax.ShapeDtypeStruct((output_weight.shape[0], size), jnp.bfloat16) for _ in cuts],
        in_specs=[hbm()] * 4 + [vmem()] * 2,
        out_specs=[vmem()] * (1 + len(cuts)),
        scratch_shapes=[
            pltpu.VMEM((length, rank), jnp.bfloat16),
            pltpu.VMEM((ROTARY, length), jnp.bfloat16),
            pltpu.VMEM((1, rank), jnp.float32),
            pltpu.SemaphoreType.DMA((3 + len(cuts),)),
        ],
        cost_estimate=pl.CostEstimate(flops=10**8, bytes_accessed=10**6, transcendentals=0),
        compiler_params=grant(60),
        name="pack",
    )(shared_latent, rotary_key.T, shared_gain[None, :], output_weight, cosine, sine)

    everyone = range(count)

    def hop(value, pairs):
        return lax.ppermute(value, "sp", pairs)

    core = [(i, i ^ 1) for i in everyone]
    ahead = [(i, i + GROUP) for i in everyone if i + GROUP < count]
    ahead_again = [(i, j) for i, j in ahead if i % GROUP > 0]
    up = [(i, i ^ 2) for i in everyone if i % GROUP < 2]
    down = [(i, i ^ 2) for i in everyone if i % GROUP >= 2]
    both = [(i, i ^ 2) for i in everyone]

    back1 = hop(mine, ahead)
    side0 = hop(mine, up)
    core0 = hop(mine, core)
    back2 = hop(back1, ahead_again)
    side1 = hop(back1, both)
    core1 = hop(back1, core)
    far0 = hop(side0, core)
    side2 = hop(back2, down)
    core2 = hop(back2, core)
    far1 = hop(side1, core)
    far2 = hop(side2, core)

    places, pieces = [], []
    if plan:
        over_z = [(i, i ^ 4) for i in everyone]
        over_y = [(i, i ^ 2) for i in everyone]
        for chunk, (base, size, kind) in enumerate(cuts):
            pulled = lax.ppermute(parts[chunk], "tp", swap)
            crossed = hop(pulled, over_z)
            if kind == "quad":
                arrived = [(0, pulled), (4, crossed)]
                arrived += [(2, hop(pulled, over_y)), (6, hop(crossed, over_y))]
            else:
                arrived = [(0, pulled), (2, crossed)]
            for change, piece in arrived:
                places.append((base, size, kind, change))
                pieces.append(piece)
                places.append((base, size, kind, change + 1))
                pieces.append(hop(piece, core))

    latents = (query_latent, query_gain[None, :], content_weight, rotary_weight, value_weight, key_weight)
    queries, value_turned, stat, acc = pl.pallas_call(
        functools.partial(begin_kernel, "sp"),
        out_shape=(
            jax.ShapeDtypeStruct((heads, length, 2 * CONTENT), jnp.bfloat16),
            jax.ShapeDtypeStruct((heads * VALUE_DIM, rank), jnp.bfloat16),
            jax.ShapeDtypeStruct((2 * heads, length), jnp.float32),
            jax.ShapeDtypeStruct((heads, VALUE_DIM, length), jnp.float32),
        ),
        in_specs=[hbm()] * 6 + [vmem()] * 4,
        out_specs=(vmem(),) * 4,
        scratch_shapes=[pltpu.VMEM(x.shape, x.dtype) for x in latents]
        + work_area(heads, length)
        + [pltpu.SemaphoreType.DMA((6,))],
        cost_estimate=pl.CostEstimate(flops=2 * 10**9, bytes_accessed=6 * 10**6, transcendentals=0),
        compiler_params=grant(58),
        name="begin",
    )(*latents, document_start[None, :], mine, cosine, sine)
    state = (stat, acc)

    def attend(state, pieces):
        stage = [place for place, _ in pieces]
        operands = [document_start, document_start[None, :], queries, key_weight, value_turned]
        operands += [array for _, array in pieces]
        aliases = {len(operands): 0, len(operands) + 1: 1}
        operands += list(state)
        return pl.pallas_call(
            functools.partial(attend_kernel, stage, "sp"),
            out_shape=(
                jax.ShapeDtypeStruct((2 * heads, length), jnp.float32),
                jax.ShapeDtypeStruct((heads, VALUE_DIM, length), jnp.float32),
            ),
            in_specs=[smem()] + [vmem()] * (len(operands) - 1),
            out_specs=(vmem(), vmem()),
            scratch_shapes=work_area(heads, length),
            input_output_aliases=aliases,
            cost_estimate=pl.CostEstimate(
                flops=10**9 * len(stage), bytes_accessed=5 * 10**6, transcendentals=0
            ),
            compiler_params=grant(18),
        )(*operands)

    state = attend(state, [(at(1, 0), core0), (at(2, 0), side0), (at(0, 4), back1)])
    state = attend(state, [(at(3, 0), far0), (at(1, 4), core1), (at(2, 4), side1)])
    state = attend(state, [(at(3, 4), far1), (at(1, 8), core2)])
    state = attend(state, [(at(2, 8), side2), (at(3, 8), far2)])

    attended = pl.pallas_call(
        functools.partial(finish_kernel, heads),
        out_shape=jax.ShapeDtypeStruct((length, heads * VALUE_DIM), jnp.bfloat16),
        in_specs=[vmem()] * 2,
        out_specs=vmem(),
        cost_estimate=pl.CostEstimate(flops=10**8, bytes_accessed=10**6, transcendentals=0),
        compiler_params=grant(8),
        name="finish",
    )(*state)

    if not plan:
        mixed = jnp.dot(attended, output_weight, preferred_element_type=jnp.float32)
        return lax.psum(mixed.astype(jnp.bfloat16), "tp")

    theirs = lax.ppermute(attended, "tp", swap)
    ours = pl.pallas_call(
        project_kernel,
        out_shape=jax.ShapeDtypeStruct((length, model), jnp.bfloat16),
        in_specs=[vmem()] * 2,
        out_specs=vmem(),
        cost_estimate=pl.CostEstimate(
            flops=2 * 10**9, bytes_accessed=10**7, transcendentals=0
        ),
        compiler_params=grant(14),
        name="ours",
    )(attended, output_weight)
    mixed = pl.pallas_call(
        functools.partial(combine_kernel, places, "sp"),
        out_shape=jax.ShapeDtypeStruct((length, model), jnp.bfloat16),
        in_specs=[vmem()] * 2 + [hbm()] * len(pieces),
        out_specs=hbm(),
        scratch_shapes=[
            pltpu.VMEM(output_weight.shape, jnp.bfloat16),
            pltpu.VMEM((length, model), jnp.bfloat16),
            pltpu.SemaphoreType.DMA((len(pieces),)),
            pltpu.SemaphoreType.DMA((len(pieces) // 2,)),
        ],
        cost_estimate=pl.CostEstimate(
            flops=2 * 10**9, bytes_accessed=10**7, transcendentals=0
        ),
        compiler_params=grant(20),
        name="theirs",
    )(theirs, ours, *pieces)
    return mixed


def solution(mesh):
    return jax.shard_map(
        on_device,
        mesh=mesh,
        in_specs=(
            P("sp", None),
            P("sp", None),
            P("sp", None),
            P("sp"),
            P(),
            P(),
            P(None, "tp"),
            P(None, "tp"),
            P(None, "tp"),
            P(None, "tp"),
            P("tp", None),
        ),
        out_specs=P("sp", None),
        check_vma=False,
    )
```

time: 106 us -> 119 us (1.12)
  the two profiles are of different devices: /device:TPU:12 before, /device:TPU:0 now
where the time goes in v1:
time: 119 us; the launch traced here: 118 us
  waiting for transfers between devices  54.9 us (46%)
  starting transfers between devices  31.6 us (27%)
  Pallas kernels  23.9 us (20%)
  local copies, waits for them, and re-layouts  6.69 us (6%)
    ppermute x3, waiting for transfers between devices, on_device(): pulled = lax.ppermute(parts[chunk], 'tp', swap)  27.2 us
    ppermute x24, starting transfers between devices, hop(): return lax.ppermute(value, 'sp', pairs)  26.5 us
    ppermute x24, waiting for transfers between devices, hop(): return lax.ppermute(value, 'sp', pairs)  21.1 us
    pallas_call x1, Pallas kernels, on_device(): pl.pallas_call(functools.partial(begin_kernel, 'sp'), out_shape=(jax.Shap...  6.96 us
    unnamed x28, local copies, waits for them, and re-layouts  6.69 us
    ppermute x1, waiting for transfers between devices, on_device(): theirs = lax.ppermute(attended, 'tp', swap)  6.59 us
    pallas_call x1, Pallas kernels, on_device(): pl.pallas_call(functools.partial(combine_kernel, places, 'sp'), out_shape...  5.7 us
    pallas_call x4, Pallas kernels, attend(): pl.pallas_call(functools.partial(attend_kernel, stage, 'sp'), out_shape=(...  3.88 us
  transfers between devices with their start and end apart: 28, of which 10 were waited for; matrix products, arithmetic and copies ran while one was open for 0% of the time, Pallas kernels for 12%

profile of v1, /device:TPU:0, one launch (start us, length us, event | category | flops | bytes accessed | tf_op | source)
XLA Modules:
  0.0 118.3 jit_solution(763097692627436553)
XLA Ops:
  0.8 3.6 %pack.1 = (bf16[288,512]{1,0:T(8,128)(2,1)}, bf16[1024,256]{1,0:T(8,128)(2,1)}, bf16[1024,256]{1,0:T(8,128)(2,1)}, bf16[1024,256]{1,0:T(8,128)(2,1)}) custom-call(bf16[256,512]{1,0:T(8,128)(2,1)} %shared_hbm.1, bf16[64,256]{1,0:T(8,128)(2,1)} %bitcast.11, f32[1,512]{1,0:T(1,128)} %bitcast.12, bf16[1024,4096]{1,0:T(8,128)(2,1)} %weight_ref.1, ...), custom_call_target="tpu_custom_call" | custom-call | flops 100000000 | bytes 1000000 | tf_op jit(solution)/shard_map/pack/pallas_call | solution.py:324
  4.4 5.0 %collective-permute-start = (bf16[288,512]{1,0:T(8,128)(2,1)}, bf16[288,512]{1,0:T(8,128)(2,1)S(1)}, u32[]{:S(2)}, u32[]{:S(2)}) collective-permute-start(bf16[288,512]{1,0:T(8,128)(2,1)} %get-tuple-element.21.refs_7_), channel_id=1, source_target_pairs={{0,8},{2,10},{4,12},{6,14},{8,16},{10,18},{12,20},{14,22},{16,24},... | collective-permute-start | bytes 884744 | tf_op jit(solution)/shard_map/ppermute | solution.py:344
  9.4 3.4 %collective-permute-start.7 = (bf16[288,512]{1,0:T(8,128)(2,1)}, bf16[288,512]{1,0:T(8,128)(2,1)S(1)}, u32[]{:S(2)}, u32[]{:S(2)}) collective-permute-start(bf16[288,512]{1,0:T(8,128)(2,1)} %get-tuple-element.21.refs_7_), channel_id=1, source_target_pairs={{0,4},{2,6},{8,12},{10,14},{16,20},{18,22},{24,28},{26,30},{1,5},{... | collective-permute-start | bytes 884744 | tf_op jit(solution)/shard_map/ppermute | solution.py:344
  12.9 1.6 %collective-permute-start.12 = (bf16[1024,256]{1,0:T(8,128)(2,1)}, bf16[1024,256]{1,0:T(8,128)(2,1)S(1)}, u32[]{:S(2)}, u32[]{:S(2)}) collective-permute-start(bf16[1024,256]{1,0:T(8,128)(2,1)} %get-tuple-element.34), channel_id=1, source_target_pairs={{0,1},{1,0},{2,3},{3,2},{4,5},{5,4},{6,7},{7,6},{8,9},{9,8},{10,11... | collective-permute-start | bytes 1572872 | tf_op jit(solution)/shard_map/ppermute | solution.py:370
  16.0 1.5 %collective-permute-start.24 = (bf16[1024,256]{1,0:T(8,128)(2,1)}, bf16[1024,256]{1,0:T(8,128)(2,1)S(1)}, u32[]{:S(2)}, u32[]{:S(2)}) collective-permute-start(bf16[1024,256]{1,0:T(8,128)(2,1)} %get-tuple-element.36), channel_id=1, source_target_pairs={{0,1},{1,0},{2,3},{3,2},{4,5},{5,4},{6,7},{7,6},{8,9},{9,8},{10,11... | collective-permute-start | bytes 1572872 | tf_op jit(solution)/shard_map/ppermute | solution.py:370
  17.5 1.7 %collective-permute-done.7.refs_6_ = bf16[288,512]{1,0:T(8,128)(2,1)S(1)} collective-permute-done((bf16[288,512]{1,0:T(8,128)(2,1)}, bf16[288,512]{1,0:T(8,128)(2,1)S(1)}, u32[]{:S(2)}, u32[]{:S(2)}) %collective-permute-start.7) | collective-permute-done | bytes 294944 | tf_op jit(solution)/shard_map/ppermute | solution.py:344
  19.1 2.4 %collective-permute-start.4 = (bf16[288,512]{1,0:T(8,128)(2,1)S(1)}, bf16[288,512]{1,0:T(8,128)(2,1)S(1)}, u32[]{:S(2)}, u32[]{:S(2)}) collective-permute-start(bf16[288,512]{1,0:T(8,128)(2,1)S(1)} %collective-permute-done.refs_7_), channel_id=1, source_target_pairs={{0,4},{2,6},{4,0},{6,2},{8,12},{10,14},{12,8},{14,10},{16,20},{18,... | collective-permute-start | bytes 884744 | tf_op jit(solution)/shard_map/ppermute | solution.py:344
  22.2 5.8 %collective-permute-done.12.refs_0_ = bf16[1024,256]{1,0:T(8,128)(2,1)S(1)} collective-permute-done((bf16[1024,256]{1,0:T(8,128)(2,1)}, bf16[1024,256]{1,0:T(8,128)(2,1)S(1)}, u32[]{:S(2)}, u32[]{:S(2)}) %collective-permute-start.12) | collective-permute-done | bytes 524320 | tf_op jit(solution)/shard_map/ppermute | solution.py:370
  28.0 11.2 %collective-permute-done.20.refs_8_ = bf16[1024,256]{1,0:T(8,128)(2,1)S(1)} collective-permute-done((bf16[1024,256]{1,0:T(8,128)(2,1)}, bf16[1024,256]{1,0:T(8,128)(2,1)S(1)}, u32[]{:S(2)}, u32[]{:S(2)}) %collective-permute-start.20) | collective-permute-done | bytes 524320 | tf_op jit(solution)/shard_map/ppermute | solution.py:370
  39.8 10.1 %collective-permute-done.24.refs_12_ = bf16[1024,256]{1,0:T(8,128)(2,1)S(1)} collective-permute-done((bf16[1024,256]{1,0:T(8,128)(2,1)}, bf16[1024,256]{1,0:T(8,128)(2,1)S(1)}, u32[]{:S(2)}, u32[]{:S(2)}) %collective-permute-start.24) | collective-permute-done | bytes 524320 | tf_op jit(solution)/shard_map/ppermute | solution.py:370
  51.3 1.6 %collective-permute-start.14 = (bf16[1024,256]{1,0:T(8,128)(2,1)S(1)}, bf16[1024,256]{1,0:T(8,128)(2,1)S(1)}, u32[]{:S(2)}, u32[]{:S(2)}) collective-permute-start(bf16[1024,256]{1,0:T(8,128)(2,1)S(1)} %collective-permute-done.12.refs_0_), channel_id=1, source_target_pairs={{0,8},{2,10},{4,12},{6,14},{8,0},{10,2},{12,4},{14,6},{16,24},{18,... | collective-permute-start | bytes 1572872 | tf_op jit(solution)/shard_map/ppermute | solution.py:344
  53.6 3.3 %collective-permute-start.16 = (bf16[1024,256]{1,0:T(8,128)(2,1)S(1)}, bf16[1024,256]{1,0:T(8,128)(2,1)S(1)}, u32[]{:S(2)}, u32[]{:S(2)}) collective-permute-start(bf16[1024,256]{1,0:T(8,128)(2,1)S(1)} %collective-permute-done.12.refs_0_), channel_id=1, source_target_pairs={{0,4},{2,6},{4,0},{6,2},{8,12},{10,14},{12,8},{14,10},{16,20},{18,... | collective-permute-start | bytes 1572872 | tf_op jit(solution)/shard_map/ppermute | solution.py:344
  58.8 1.6 %collective-permute-start.26 = (bf16[1024,256]{1,0:T(8,128)(2,1)S(1)}, bf16[1024,256]{1,0:T(8,128)(2,1)S(1)}, u32[]{:S(2)}, u32[]{:S(2)}) collective-permute-start(bf16[1024,256]{1,0:T(8,128)(2,1)S(1)} %collective-permute-done.24.refs_12_), channel_id=1, source_target_pairs={{0,8},{2,10},{4,12},{6,14},{8,0},{10,2},{12,4},{14,6},{16,24},{18,... | collective-permute-start | bytes 1572872 | tf_op jit(solution)/shard_map/ppermute | solution.py:344
  60.4 1.4 %collective-permute-done.2.refs_5_ = bf16[288,512]{1,0:T(8,128)(2,1)} collective-permute-done((bf16[288,512]{1,0:T(8,128)(2,1)S(1)}, bf16[288,512]{1,0:T(8,128)(2,1)}, u32[]{:S(2)}, u32[]{:S(2)}) %collective-permute-start.2) | collective-permute-done | bytes 294944 | tf_op jit(solution)/shard_map/ppermute | solution.py:344
  61.8 7.0 %begin.1 = (bf16[8,256,256]{2,1,0:T(8,128)(2,1)}, bf16[1024,512]{1,0:T(8,128)(2,1)}, f32[16,256]{1,0:T(8,128)}, f32[8,128,256]{2,1,0:T(8,128)}) custom-call(bf16[256,1024]{1,0:T(8,128)(2,1)} %refs_0_.5, f32[1,1024]{1,0:T(1,128)} %bitcast.13, bf16[1024,1024]{1,0:T(8,128)(2,1)} %refs_2_.1, bf16[1024,512]{1,0:T(8,128)(2,1)} %refs_3_.5, ...), custom_call_target="tpu_custom_call" | custom-call | flops 2000000000 | bytes 6000000 | tf_op jit(solution)/shard_map/begin/pallas_call | solution.py:384
  73.9 2.0 %collective-permute-start.13 = (bf16[1024,256]{1,0:T(8,128)(2,1)S(1)}, bf16[1024,256]{1,0:T(8,128)(2,1)S(1)}, u32[]{:S(2)}, u32[]{:S(2)}) collective-permute-start(bf16[1024,256]{1,0:T(8,128)(2,1)S(1)} %collective-permute-done.12.refs_0_), channel_id=1, source_target_pairs={{0,2},{2,0},{4,6},{6,4},{8,10},{10,8},{12,14},{14,12},{16,18},{18,... | collective-permute-start | bytes 1572872 | tf_op jit(solution)/shard_map/ppermute | solution.py:344
  77.4 9.8 %collective-permute-done.26.refs_14_ = bf16[1024,256]{1,0:T(8,128)(2,1)S(1)} collective-permute-done((bf16[1024,256]{1,0:T(8,128)(2,1)S(1)}, bf16[1024,256]{1,0:T(8,128)(2,1)S(1)}, u32[]{:S(2)}, u32[]{:S(2)}) %collective-permute-start.26) | collective-permute-done | bytes 524320 | tf_op jit(solution)/shard_map/ppermute | solution.py:344
  87.2 3.0 %collective-permute-start.18 = (bf16[1024,256]{1,0:T(8,128)(2,1)S(1)}, bf16[1024,256]{1,0:T(8,128)(2,1)S(1)}, u32[]{:S(2)}, u32[]{:S(2)}) collective-permute-start(bf16[1024,256]{1,0:T(8,128)(2,1)S(1)} %collective-permute-done.14.refs_2_), channel_id=1, source_target_pairs={{0,4},{2,6},{4,0},{6,2},{8,12},{10,14},{12,8},{14,10},{16,20},{18,... | collective-permute-start | bytes 1572872 | tf_op jit(solution)/shard_map/ppermute | solution.py:344
  92.0 1.6 %shard_map.112 = (f32[16,256]{1,0:T(8,128)S(1)}, f32[8,128,256]{2,1,0:T(8,128)S(1)}) custom-call(s32[256]{0:T(256)S(1)} %copy-done.9, s32[1,256]{1,0:T(1,128)S(1)} %bitcast.10, bf16[8,256,256]{2,1,0:T(8,128)(2,1)S(1)} %copy-done.10, bf16[512,1024]{1,0:T(8,128)(2,1)S(1)} %copy-done.2, ...), custom_call_target="tpu_custom_call", output_to_operand_aliasing={{0}: (7, {}), {1}: (8, {})} | custom-call | flops 2000000000 | bytes 5000000 | tf_op jit(solution)/shard_map/pallas_call | solution.py:409
  94.9 5.8 %collective-permute-done.18.refs_6_ = bf16[1024,256]{1,0:T(8,128)(2,1)S(1)} collective-permute-done((bf16[1024,256]{1,0:T(8,128)(2,1)S(1)}, bf16[1024,256]{1,0:T(8,128)(2,1)S(1)}, u32[]{:S(2)}, u32[]{:S(2)}) %collective-permute-start.18) | collective-permute-done | bytes 524320 | tf_op jit(solution)/shard_map/ppermute | solution.py:344
  100.7 1.5 %collective-permute-start.11 = (bf16[256,1024]{1,0:T(8,128)(2,1)S(1)}, bf16[256,1024]{1,0:T(8,128)(2,1)S(1)}, u32[]{:S(2)}, u32[]{:S(2)}) collective-permute-start(bf16[256,1024]{1,0:T(8,128)(2,1)S(1)} %finish.1.rows_ref), channel_id=1, source_target_pairs={{0,1},{1,0},{2,3},{3,2},{4,5},{5,4},{6,7},{7,6},{8,9},{9,8},{10,11... | collective-permute-start | bytes 1572872 | tf_op jit(solution)/shard_map/ppermute | solution.py:444
  102.3 3.5 %ours.1.ours_ref = bf16[256,4096]{1,0:T(8,128)(2,1)S(1)} custom-call(bf16[256,1024]{1,0:T(8,128)(2,1)S(1)} %finish.1.rows_ref, bf16[1024,4096]{1,0:T(8,128)(2,1)S(1)} %bitcast.5), custom_call_target="tpu_custom_call" | custom-call | flops 2000000000 | bytes 10000000 | tf_op jit(solution)/shard_map/ours/pallas_call | solution.py:445
  105.8 6.6 %collective-permute-done.11.rows_ref = bf16[256,1024]{1,0:T(8,128)(2,1)S(1)} collective-permute-done((bf16[256,1024]{1,0:T(8,128)(2,1)S(1)}, bf16[256,1024]{1,0:T(8,128)(2,1)S(1)}, u32[]{:S(2)}, u32[]{:S(2)}) %collective-permute-start.11) | collective-permute-done | bytes 524320 | tf_op jit(solution)/shard_map/ppermute | solution.py:444
  112.4 5.7 %theirs.1 = bf16[256,4096]{1,0:T(8,128)(2,1)} custom-call(bf16[256,1024]{1,0:T(8,128)(2,1)S(1)} %collective-permute-done.11.rows_ref, bf16[256,4096]{1,0:T(8,128)(2,1)S(1)} %ours.1.ours_ref, bf16[1024,256]{1,0:T(8,128)(2,1)S(1)} %collective-permute-done.12.refs_0_, bf16[1024,256]{1,0:T(8,128)(2,1)S(1)} %collective-permute-done.13.refs_1_, ...), custom_call_target="tpu_custom_call" | custom-call | flops 2000000000 | bytes 10000000 | tf_op jit(solution)/shard_map/theirs/pallas_call | solution.py:456
  (73 shorter events, 17.2 us)
Async XLA Ops:
  4.4 11.5 %collective-permute-start = (bf16[288,512]{1,0:T(8,128)(2,1)}, bf16[288,512]{1,0:T(8,128)(2,1)S(1)}, u32[]{:S(2)}, u32[]{:S(2)}) collective-permute-start(bf16[288,512]{1,0:T(8,128)(2,1)} %get-tuple-element.21.refs_7_), channel_id=1, source_target_pairs={{0,8},{2,10},{4,12},{6,14},{8,16},{10,18},{12,20},{14,22},{16,24},... | collective-permute-start | bytes 884744 | tf_op jit(solution)/shard_map/ppermute | solution.py:344
  12.9 15.1 %collective-permute-start.12 = (bf16[1024,256]{1,0:T(8,128)(2,1)}, bf16[1024,256]{1,0:T(8,128)(2,1)S(1)}, u32[]{:S(2)}, u32[]{:S(2)}) collective-permute-start(bf16[1024,256]{1,0:T(8,128)(2,1)} %get-tuple-element.34), channel_id=1, source_target_pairs={{0,1},{1,0},{2,3},{3,2},{4,5},{5,4},{6,7},{7,6},{8,9},{9,8},{10,11... | collective-permute-start | bytes 1572872 | tf_op jit(solution)/shard_map/ppermute | solution.py:370
  14.5 24.8 %collective-permute-start.20 = (bf16[1024,256]{1,0:T(8,128)(2,1)}, bf16[1024,256]{1,0:T(8,128)(2,1)S(1)}, u32[]{:S(2)}, u32[]{:S(2)}) collective-permute-start(bf16[1024,256]{1,0:T(8,128)(2,1)} %get-tuple-element.35), channel_id=1, source_target_pairs={{0,1},{1,0},{2,3},{3,2},{4,5},{5,4},{6,7},{7,6},{8,9},{9,8},{10,11... | collective-permute-start | bytes 1572872 | tf_op jit(solution)/shard_map/ppermute | solution.py:370
  16.0 34.0 %collective-permute-start.24 = (bf16[1024,256]{1,0:T(8,128)(2,1)}, bf16[1024,256]{1,0:T(8,128)(2,1)S(1)}, u32[]{:S(2)}, u32[]{:S(2)}) collective-permute-start(bf16[1024,256]{1,0:T(8,128)(2,1)} %get-tuple-element.36), channel_id=1, source_target_pairs={{0,1},{1,0},{2,3},{3,2},{4,5},{5,4},{6,7},{7,6},{8,9},{9,8},{10,11... | collective-permute-start | bytes 1572872 | tf_op jit(solution)/shard_map/ppermute | solution.py:370
  19.1 20.1 %collective-permute-start.4 = (bf16[288,512]{1,0:T(8,128)(2,1)S(1)}, bf16[288,512]{1,0:T(8,128)(2,1)S(1)}, u32[]{:S(2)}, u32[]{:S(2)}) collective-permute-start(bf16[288,512]{1,0:T(8,128)(2,1)S(1)} %collective-permute-done.refs_7_), channel_id=1, source_target_pairs={{0,4},{2,6},{4,0},{6,2},{8,12},{10,14},{12,8},{14,10},{16,20},{18,... | collective-permute-start | bytes 884744 | tf_op jit(solution)/shard_map/ppermute | solution.py:344
  21.5 18.3 %collective-permute-start.1 = (bf16[288,512]{1,0:T(8,128)(2,1)S(1)}, bf16[288,512]{1,0:T(8,128)(2,1)S(1)}, u32[]{:S(2)}, u32[]{:S(2)}) collective-permute-start(bf16[288,512]{1,0:T(8,128)(2,1)S(1)} %collective-permute-done.refs_7_), channel_id=1, source_target_pairs={{2,10},{4,12},{6,14},{10,18},{12,20},{14,22},{18,26},{20,28},{22,3... | collective-permute-start | bytes 884744 | tf_op jit(solution)/shard_map/ppermute | solution.py:344
  28.0 23.2 %collective-permute-start.9 = (bf16[288,512]{1,0:T(8,128)(2,1)S(1)}, bf16[288,512]{1,0:T(8,128)(2,1)S(1)}, u32[]{:S(2)}, u32[]{:S(2)}) collective-permute-start(bf16[288,512]{1,0:T(8,128)(2,1)S(1)} %collective-permute-done.refs_7_), channel_id=1, source_target_pairs={{0,2},{2,0},{4,6},{6,4},{8,10},{10,8},{12,14},{14,12},{16,18},{18,... | collective-permute-start | bytes 884744 | tf_op jit(solution)/shard_map/ppermute | solution.py:344
  39.3 13.6 %collective-permute-start.8 = (bf16[288,512]{1,0:T(8,128)(2,1)S(1)}, bf16[288,512]{1,0:T(8,128)(2,1)S(1)}, u32[]{:S(2)}, u32[]{:S(2)}) collective-permute-start(bf16[288,512]{1,0:T(8,128)(2,1)S(1)} %collective-permute-done.7.refs_6_), channel_id=1, source_target_pairs={{0,2},{2,0},{4,6},{6,4},{8,10},{10,8},{12,14},{14,12},{16,18},{18,... | collective-permute-start | bytes 884744 | tf_op jit(solution)/shard_map/ppermute | solution.py:344
  39.3 17.7 %collective-permute-start.5 = (bf16[288,512]{1,0:T(8,128)(2,1)S(1)}, bf16[288,512]{1,0:T(8,128)(2,1)S(1)}, u32[]{:S(2)}, u32[]{:S(2)}) collective-permute-start(bf16[288,512]{1,0:T(8,128)(2,1)S(1)} %collective-permute-done.4.refs_7_), channel_id=1, source_target_pairs={{0,2},{2,0},{4,6},{6,4},{8,10},{10,8},{12,14},{14,12},{16,18},{18,... | collective-permute-start | bytes 884744 | tf_op jit(solution)/shard_map/ppermute | solution.py:344
  39.8 18.3 %collective-permute-start.6 = (bf16[288,512]{1,0:T(8,128)(2,1)S(1)}, bf16[288,512]{1,0:T(8,128)(2,1)S(1)}, u32[]{:S(2)}, u32[]{:S(2)}) collective-permute-start(bf16[288,512]{1,0:T(8,128)(2,1)S(1)} %collective-permute-done.1), channel_id=1, source_target_pairs={{0,2},{2,0},{4,6},{6,4},{8,10},{10,8},{12,14},{14,12},{16,18},{18,... | collective-permute-start | bytes 884744 | tf_op jit(solution)/shard_map/ppermute | solution.py:344
  50.0 11.9 %collective-permute-start.2 = (bf16[288,512]{1,0:T(8,128)(2,1)S(1)}, bf16[288,512]{1,0:T(8,128)(2,1)}, u32[]{:S(2)}, u32[]{:S(2)}) collective-permute-start(bf16[288,512]{1,0:T(8,128)(2,1)S(1)} %collective-permute-done.1), channel_id=1, source_target_pairs={{4,0},{6,2},{12,8},{14,10},{20,16},{22,18},{28,24},{30,26},{5,1},{... | collective-permute-start | bytes 884744 | tf_op jit(solution)/shard_map/ppermute | solution.py:344
  51.3 22.7 %collective-permute-start.14 = (bf16[1024,256]{1,0:T(8,128)(2,1)S(1)}, bf16[1024,256]{1,0:T(8,128)(2,1)S(1)}, u32[]{:S(2)}, u32[]{:S(2)}) collective-permute-start(bf16[1024,256]{1,0:T(8,128)(2,1)S(1)} %collective-permute-done.12.refs_0_), channel_id=1, source_target_pairs={{0,8},{2,10},{4,12},{6,14},{8,0},{10,2},{12,4},{14,6},{16,24},{18,... | collective-permute-start | bytes 1572872 | tf_op jit(solution)/shard_map/ppermute | solution.py:344
  53.6 22.3 %collective-permute-start.16 = (bf16[1024,256]{1,0:T(8,128)(2,1)S(1)}, bf16[1024,256]{1,0:T(8,128)(2,1)S(1)}, u32[]{:S(2)}, u32[]{:S(2)}) collective-permute-start(bf16[1024,256]{1,0:T(8,128)(2,1)S(1)} %collective-permute-done.12.refs_0_), channel_id=1, source_target_pairs={{0,4},{2,6},{4,0},{6,2},{8,12},{10,14},{12,8},{14,10},{16,20},{18,... | collective-permute-start | bytes 1572872 | tf_op jit(solution)/shard_map/ppermute | solution.py:344
  57.6 19.7 %collective-permute-start.22 = (bf16[1024,256]{1,0:T(8,128)(2,1)S(1)}, bf16[1024,256]{1,0:T(8,128)(2,1)S(1)}, u32[]{:S(2)}, u32[]{:S(2)}) collective-permute-start(bf16[1024,256]{1,0:T(8,128)(2,1)S(1)} %collective-permute-done.20.refs_8_), channel_id=1, source_target_pairs={{0,8},{2,10},{4,12},{6,14},{8,0},{10,2},{12,4},{14,6},{16,24},{18,... | collective-permute-start | bytes 1572872 | tf_op jit(solution)/shard_map/ppermute | solution.py:344
  58.8 28.4 %collective-permute-start.26 = (bf16[1024,256]{1,0:T(8,128)(2,1)S(1)}, bf16[1024,256]{1,0:T(8,128)(2,1)S(1)}, u32[]{:S(2)}, u32[]{:S(2)}) collective-permute-start(bf16[1024,256]{1,0:T(8,128)(2,1)S(1)} %collective-permute-done.24.refs_12_), channel_id=1, source_target_pairs={{0,8},{2,10},{4,12},{6,14},{8,0},{10,2},{12,4},{14,6},{16,24},{18,... | collective-permute-start | bytes 1572872 | tf_op jit(solution)/shard_map/ppermute | solution.py:344
  61.8 28.4 %collective-permute-start.3 = (bf16[288,512]{1,0:T(8,128)(2,1)}, bf16[288,512]{1,0:T(8,128)(2,1)}, u32[]{:S(2)}, u32[]{:S(2)}) collective-permute-start(bf16[288,512]{1,0:T(8,128)(2,1)} %collective-permute-done.2.refs_5_), channel_id=1, source_target_pairs={{0,2},{2,0},{4,6},{6,4},{8,10},{10,8},{12,14},{14,12},{16,18},{18,... | collective-permute-start | bytes 884744 | tf_op jit(solution)/shard_map/ppermute | solution.py:344
  73.9 19.9 %collective-permute-start.13 = (bf16[1024,256]{1,0:T(8,128)(2,1)S(1)}, bf16[1024,256]{1,0:T(8,128)(2,1)S(1)}, u32[]{:S(2)}, u32[]{:S(2)}) collective-permute-start(bf16[1024,256]{1,0:T(8,128)(2,1)S(1)} %collective-permute-done.12.refs_0_), channel_id=1, source_target_pairs={{0,2},{2,0},{4,6},{6,4},{8,10},{10,8},{12,14},{14,12},{16,18},{18,... | collective-permute-start | bytes 1572872 | tf_op jit(solution)/shard_map/ppermute | solution.py:344
  75.9 18.5 %collective-permute-start.21 = (bf16[1024,256]{1,0:T(8,128)(2,1)S(1)}, bf16[1024,256]{1,0:T(8,128)(2,1)S(1)}, u32[]{:S(2)}, u32[]{:S(2)}) collective-permute-start(bf16[1024,256]{1,0:T(8,128)(2,1)S(1)} %collective-permute-done.20.refs_8_), channel_id=1, source_target_pairs={{0,2},{2,0},{4,6},{6,4},{8,10},{10,8},{12,14},{14,12},{16,18},{18,... | collective-permute-start | bytes 1572872 | tf_op jit(solution)/shard_map/ppermute | solution.py:344
  77.3 17.1 %collective-permute-start.25 = (bf16[1024,256]{1,0:T(8,128)(2,1)S(1)}, bf16[1024,256]{1,0:T(8,128)(2,1)S(1)}, u32[]{:S(2)}, u32[]{:S(2)}) collective-permute-start(bf16[1024,256]{1,0:T(8,128)(2,1)S(1)} %collective-permute-done.24.refs_12_), channel_id=1, source_target_pairs={{0,2},{2,0},{4,6},{6,4},{8,10},{10,8},{12,14},{14,12},{16,18},{18,... | collective-permute-start | bytes 1572872 | tf_op jit(solution)/shard_map/ppermute | solution.py:344
  87.2 13.6 %collective-permute-start.18 = (bf16[1024,256]{1,0:T(8,128)(2,1)S(1)}, bf16[1024,256]{1,0:T(8,128)(2,1)S(1)}, u32[]{:S(2)}, u32[]{:S(2)}) collective-permute-start(bf16[1024,256]{1,0:T(8,128)(2,1)S(1)} %collective-permute-done.14.refs_2_), channel_id=1, source_target_pairs={{0,4},{2,6},{4,0},{6,2},{8,12},{10,14},{12,8},{14,10},{16,20},{18,... | collective-permute-start | bytes 1572872 | tf_op jit(solution)/shard_map/ppermute | solution.py:344
  90.2 12.0 %collective-permute-start.15 = (bf16[1024,256]{1,0:T(8,128)(2,1)S(1)}, bf16[1024,256]{1,0:T(8,128)(2,1)S(1)}, u32[]{:S(2)}, u32[]{:S(2)}) collective-permute-start(bf16[1024,256]{1,0:T(8,128)(2,1)S(1)} %collective-permute-done.14.refs_2_), channel_id=1, source_target_pairs={{0,2},{2,0},{4,6},{6,4},{8,10},{10,8},{12,14},{14,12},{16,18},{18,... | collective-permute-start | bytes 1572872 | tf_op jit(solution)/shard_map/ppermute | solution.py:344
  93.8 12.0 %collective-permute-start.17 = (bf16[1024,256]{1,0:T(8,128)(2,1)S(1)}, bf16[1024,256]{1,0:T(8,128)(2,1)S(1)}, u32[]{:S(2)}, u32[]{:S(2)}) collective-permute-start(bf16[1024,256]{1,0:T(8,128)(2,1)S(1)} %collective-permute-done.16.refs_4_), channel_id=1, source_target_pairs={{0,2},{2,0},{4,6},{6,4},{8,10},{10,8},{12,14},{14,12},{16,18},{18,... | collective-permute-start | bytes 1572872 | tf_op jit(solution)/shard_map/ppermute | solution.py:344
  94.4 11.4 %collective-permute-start.23 = (bf16[1024,256]{1,0:T(8,128)(2,1)S(1)}, bf16[1024,256]{1,0:T(8,128)(2,1)S(1)}, u32[]{:S(2)}, u32[]{:S(2)}) collective-permute-start(bf16[1024,256]{1,0:T(8,128)(2,1)S(1)} %collective-permute-done.22.refs_10_), channel_id=1, source_target_pairs={{0,2},{2,0},{4,6},{6,4},{8,10},{10,8},{12,14},{14,12},{16,18},{18,... | collective-permute-start | bytes 1572872 | tf_op jit(solution)/shard_map/ppermute | solution.py:344
  100.7 11.7 %collective-permute-start.11 = (bf16[256,1024]{1,0:T(8,128)(2,1)S(1)}, bf16[256,1024]{1,0:T(8,128)(2,1)S(1)}, u32[]{:S(2)}, u32[]{:S(2)}) collective-permute-start(bf16[256,1024]{1,0:T(8,128)(2,1)S(1)} %finish.1.rows_ref), channel_id=1, source_target_pairs={{0,1},{1,0},{2,3},{3,2},{4,5},{5,4},{6,7},{7,6},{8,9},{9,8},{10,11... | collective-permute-start | bytes 1572872 | tf_op jit(solution)/shard_map/ppermute | solution.py:444
  (18 other events, 100.6 us)

commit v2 on v1

--- a/solution.py
+++ b/solution.py
@@ -11,7 +11,8 @@
 ROTARY = 64
 VALUE_DIM = 128
 GROUP = 4
-KINDS = ("quad", "pair", "pair")
+KINDS = (("quad", 1), ("z", 2), ("y", 2), ("z", 2))
+EARLY = 16
 
 norm_eps = 1e-06
 rope_theta = 10000.0
@@ -57,18 +58,20 @@
     return copies
 
 
-def pack_kernel(cuts, axis, shared_hbm, rotary_hbm, gain_hbm, weight_hbm, cos_ref, sin_ref, *refs):
-    out_ref, parts, refs = refs[0], refs[1 : 1 + len(cuts)], refs[1 + len(cuts) :]
-    shared_ref, rotary_ref, gain_ref, sems = refs
-    length, rank = shared_ref.shape
-    half = ROTARY // 2
+def cut_kernel(cuts, axis, weight_hbm, *refs):
+    parts, sems = refs[:-1], refs[-1]
     me = lax.axis_index(axis)
-    pairs = [(rotary_hbm, rotary_ref), (gain_hbm, gain_ref), (shared_hbm, shared_ref)]
+    pairs = []
     for (base, size, kind), part_ref in zip(cuts, parts):
         start = pl.multiple_of(base + slot_of(me, kind) * size, 128)
         pairs.append((weight_hbm.at[:, pl.ds(start, size)], part_ref))
-    copies = load(pairs, sems)
-    copies[0].wait()
+    for copy in load(pairs, sems):
+        copy.wait()
+
+
+def pack_kernel(shared_ref, rotary_ref, gain_ref, cos_ref, sin_ref, out_ref):
+    length, rank = shared_ref.shape
+    half = ROTARY // 2
     key = rotary_ref[...].astype(jnp.float32)
     low, high = key[:half], key[half:]
     cosine, sine = cos_ref[...], sin_ref[...]
@@ -82,33 +85,22 @@
         out_ref[length:, pair * 2 * ROTARY : (pair + 1) * 2 * ROTARY] = jnp.where(
             lane < ROTARY, low, high
         ).astype(jnp.bfloat16)
-    copies[1].wait()
-    copies[2].wait()
     out_ref[0:length, :] = normed(shared_ref[...], gain_ref[...])
-    for copy in copies[3:]:
-        copy.wait()
 
 
 def begin_kernel(axis, *refs):
-    hbm, refs = refs[:6], refs[6:]
-    starts_ref, block_ref, cos_ref, sin_ref = refs[:4]
-    query_ref, turned_value_ref, stat_ref, acc_ref = refs[4:8]
-    held, refs = refs[8:14], refs[14:]
-    scratch, sems = refs[:-1], refs[-1]
-    copies = load(list(zip(hbm, held)), sems)
-    latent_ref, gain_ref, content_ref, rotary_ref, value_ref, key_ref = held
+    latent_ref, gain_ref, content_ref, rotary_ref, value_ref, key_ref = refs[:6]
+    starts_ref, block_ref, cos_ref, sin_ref = refs[6:10]
+    query_ref, turned_value_ref, stat_ref, acc_ref = refs[10:14]
+    scratch = refs[14:]
     cos4 = jnp.concatenate([cos_ref[...]] * 4, axis=0).T
     sin4 = jnp.concatenate([-sin_ref[...], sin_ref[...]] * 2, axis=0).T
-    copies[0].wait()
-    copies[1].wait()
     rows = normed(latent_ref[...], gain_ref[...])
-    copies[2].wait()
     content = jnp.dot(rows, content_ref[...], preferred_element_type=jnp.float32)
     for head in range(query_ref.shape[0]):
         query_ref[head, :, 0:CONTENT] = content[:, head * CONTENT : (head + 1) * CONTENT].astype(
             jnp.bfloat16
         )
-    copies[3].wait()
     raw = jnp.dot(rows, rotary_ref[...], preferred_element_type=jnp.float32)
     lane = lax.broadcasted_iota(jnp.int32, (rows.shape[0], 2 * ROTARY), 1)
     for pair in range(query_ref.shape[0] // 2):
@@ -119,9 +111,7 @@
             query_ref[2 * pair + side, :, CONTENT:] = jnp.where(own, turned, 0.0).astype(
                 jnp.bfloat16
             )
-    copies[4].wait()
     turned_value_ref[...] = value_ref[...].T
-    copies[5].wait()
     me = lax.axis_index(axis)
     absorb(
         me, me, True, block_ref, starts_ref, query_ref, key_ref, turned_value_ref, stat_ref, acc_ref, *scratch
@@ -249,36 +239,39 @@
 def slot_of(me, kind):
     if kind == "quad":
         return jnp.bitwise_and(me, 7)
-    return jnp.bitwise_and(lax.shift_right_logical(me, 2), 1) * 2 + jnp.bitwise_and(me, 1)
+    bit = 2 if kind == "z" else 1
+    return jnp.bitwise_and(lax.shift_right_logical(me, bit), 1) * 2 + jnp.bitwise_and(me, 1)
 
 
 def combine_kernel(places, axis, rows_ref, ours_ref, *refs):
     me = lax.axis_index(axis)
     count = len(places)
-    pieces, out_hbm, refs = refs[:count], refs[count], refs[count + 1 :]
-    held_ref, done_ref, sems, out_sems = refs
-    copies = []
-    for k, (base, size, kind, change) in enumerate(places):
-        start = base + jnp.bitwise_xor(slot_of(me, kind), change) * size
-        columns = pl.ds(pl.multiple_of(start, 128), size)
-        copies.append(pltpu.make_async_copy(pieces[k], held_ref.at[:, columns], sems.at[k]))
-    ahead = 6
-    for copy in copies[:ahead]:
-        copy.start()
+    pieces, (out_hbm, done_ref, out_sems) = refs[:count], refs[-3:]
+    rows = rows_ref[...]
     leaving = []
     for k in range(0, count, 2):
         base, size, kind, change = places[k]
+        starts = [
+            pl.multiple_of(base + jnp.bitwise_xor(slot_of(me, kind), flip) * size, 128)
+            for flip in (change, change + 1)
+        ]
+        if size % 256 == 0:
+            terms = [
+                jnp.dot(rows, pieces[j][...], preferred_element_type=jnp.float32)
+                for j in (k, k + 1)
+            ]
+        else:
+            both = jnp.concatenate([pieces[k][...], pieces[k + 1][...]], axis=1)
+            term = jnp.dot(rows, both, preferred_element_type=jnp.float32)
+            terms = [term[:, :size], term[:, size:]]
+        for start, term in zip(starts, terms):
+            columns = pl.ds(start, size)
+            term = term.astype(jnp.bfloat16).astype(jnp.float32)
+            done_ref[:, columns] = (ours_ref[:, columns].astype(jnp.float32) + term).astype(
+                jnp.bfloat16
+            )
         start = base + (jnp.bitwise_xor(slot_of(me, kind), change) // 2) * (2 * size)
         columns = pl.ds(pl.multiple_of(start, 256), 2 * size)
-        for late in (k, k + 1):
-            copies[late].wait()
-            if late + ahead < count:
-                copies[late + ahead].start()
-        term = jnp.dot(rows_ref[...], held_ref[:, columns], preferred_element_type=jnp.float32)
-        term = term.astype(jnp.bfloat16).astype(jnp.float32)
-        done_ref[:, columns] = (ours_ref[:, columns].astype(jnp.float32) + term).astype(
-            jnp.bfloat16
-        )
         out = pltpu.make_async_copy(
             done_ref.at[:, columns], out_hbm.at[:, columns], out_sems.at[k // 2]
         )
@@ -312,31 +305,40 @@
     angles = frequency[:, None] * position[None, :]
     cosine, sine = jnp.cos(angles), jnp.sin(angles)
 
-    plan = groups == 2 and count % 8 == 0 and model % 2048 == 0
+    plan = groups == 2 and count % 8 == 0 and model % 4096 == 0
     swap = [(0, 1), (1, 0)]
-    size = model // 16
     cuts, base = [], 0
-    for kind in KINDS if plan else ():
+    for kind, share in KINDS if plan else ():
+        size = share * model // 32
         cuts.append((base, size, kind))
         base += size * (8 if kind == "quad" else 4)
 
     packed_rows = length + length * ROTARY // rank
-    mine, *parts = pl.pallas_call(
-        functools.partial(pack_kernel, cuts, "sp"),
-        out_shape=[jax.ShapeDtypeStruct((packed_rows, rank), jnp.bfloat16)]
-        + [jax.ShapeDtypeStruct((output_weight.shape[0], size), jnp.bfloat16) for _ in cuts],
-        in_specs=[hbm()] * 4 + [vmem()] * 2,
-        out_specs=[vmem()] * (1 + len(cuts)),
-        scratch_shapes=[
-            pltpu.VMEM((length, rank), jnp.bfloat16),
-            pltpu.VMEM((ROTARY, length), jnp.bfloat16),
-            pltpu.VMEM((1, rank), jnp.float32),
-            pltpu.SemaphoreType.DMA((3 + len(cuts),)),
-        ],
-        cost_estimate=pl.CostEstimate(flops=10**8, bytes_accessed=10**6, transcendentals=0),
-        compiler_params=grant(60),
+    if plan:
+        parts = pl.pallas_call(
+            functools.partial(cut_kernel, cuts, "sp"),
+            out_shape=[
+                jax.ShapeDtypeStruct((output_weight.shape[0], size), jnp.bfloat16)
+                for _, size, _ in cuts
+            ],
+            in_specs=[hbm()],
+            out_specs=[vmem()] * len(cuts),
+            scratch_shapes=[pltpu.SemaphoreType.DMA((len(cuts),))],
+            cost_estimate=pl.CostEstimate(
+                flops=10**8, bytes_accessed=10**7, transcendentals=0
+            ),
+            compiler_params=grant(57),
+            name="cut",
+        )(output_weight)
+    mine = pl.pallas_call(
+        pack_kernel,
+        out_shape=jax.ShapeDtypeStruct((packed_rows, rank), jnp.bfloat16),
+        in_specs=[vmem()] * 5,
+        out_specs=vmem(),
+        cost_estimate=pl.CostEstimate(flops=2 * 10**10, bytes_accessed=2 * 10**7, transcendentals=0),
+        compiler_params=grant(8),
         name="pack",
-    )(shared_latent, rotary_key.T, shared_gain[None, :], output_weight, cosine, sine)
+    )(shared_latent, rotary_key.T, shared_gain[None, :], cosine, sine)
 
     everyone = range(count)
 
@@ -368,7 +370,7 @@
         over_y = [(i, i ^ 2) for i in everyone]
         for chunk, (base, size, kind) in enumerate(cuts):
             pulled = lax.ppermute(parts[chunk], "tp", swap)
-            crossed = hop(pulled, over_z)
+            crossed = hop(pulled, over_y if kind == "y" else over_z)
             if kind == "quad":
                 arrived = [(0, pulled), (4, crossed)]
                 arrived += [(2, hop(pulled, over_y)), (6, hop(crossed, over_y))]
@@ -389,13 +391,11 @@
             jax.ShapeDtypeStruct((2 * heads, length), jnp.float32),
             jax.ShapeDtypeStruct((heads, VALUE_DIM, length), jnp.float32),
         ),
-        in_specs=[hbm()] * 6 + [vmem()] * 4,
+        in_specs=[vmem()] * 10,
         out_specs=(vmem(),) * 4,
-        scratch_shapes=[pltpu.VMEM(x.shape, x.dtype) for x in latents]
-        + work_area(heads, length)
-        + [pltpu.SemaphoreType.DMA((6,))],
+        scratch_shapes=work_area(heads, length),
         cost_estimate=pl.CostEstimate(flops=2 * 10**9, bytes_accessed=6 * 10**6, transcendentals=0),
-        compiler_params=grant(58),
+        compiler_params=grant(14),
         name="begin",
     )(*latents, document_start[None, :], mine, cosine, sine)
     state = (stat, acc)
@@ -453,23 +453,27 @@
         compiler_params=grant(14),
         name="ours",
     )(attended, output_weight)
-    mixed = pl.pallas_call(
-        functools.partial(combine_kernel, places, "sp"),
-        out_shape=jax.ShapeDtypeStruct((length, model), jnp.bfloat16),
-        in_specs=[vmem()] * 2 + [hbm()] * len(pieces),
-        out_specs=hbm(),
-        scratch_shapes=[
-            pltpu.VMEM(output_weight.shape, jnp.bfloat16),
-            pltpu.VMEM((length, model), jnp.bfloat16),
-            pltpu.SemaphoreType.DMA((len(pieces),)),
-            pltpu.SemaphoreType.DMA((len(pieces) // 2,)),
-        ],
-        cost_estimate=pl.CostEstimate(
-            flops=2 * 10**9, bytes_accessed=10**7, transcendentals=0
-        ),
-        compiler_params=grant(20),
-        name="theirs",
-    )(theirs, ours, *pieces)
+    mixed = None
+    for low, high in ((0, EARLY), (EARLY, len(pieces))):
+        operands = [theirs, ours, *pieces[low:high]]
+        aliases = {}
+        if mixed is not None:
+            aliases = {len(operands): 0}
+            operands.append(mixed)
+        mixed = pl.pallas_call(
+            functools.partial(combine_kernel, places[low:high], "sp"),
+            out_shape=jax.ShapeDtypeStruct((length, model), jnp.bfloat16),
+            in_specs=[vmem()] * (2 + high - low)
+            + [hbm()] * (len(operands) - 2 - high + low),
+            out_specs=hbm(),
+            scratch_shapes=[
+                pltpu.VMEM((length, model), jnp.bfloat16),
+                pltpu.SemaphoreType.DMA(((high - low) // 2,)),
+            ],
+            input_output_aliases=aliases,
+            cost_estimate=pl.CostEstimate(flops=10**9, bytes_accessed=5 * 10**6, transcendentals=0),
+            compiler_params=grant(14),
+        )(*operands)
     return mixed
 
 

time: 119 us -> 102 us (0.86)
  Pallas kernels: 23.9 us -> 16.4 us
  starting transfers between devices: 31.6 us -> 27.3 us
  local copies, waits for them, and re-layouts: 6.69 us -> 2.44 us
    ppermute x1, waiting for transfers between devices: 6.59 us -> 1.67 us  [on_device(): theirs = lax.ppermute(attended, 'tp', swap)]
    ppermute x24 -> x27, starting transfers between devices: 26.5 us -> 21.7 us  [hop(): return lax.ppermute(value, 'sp', pairs)]
    pallas_call x1, Pallas kernels: 6.96 us -> 2.44 us  [on_device(): pl.pallas_call(functools.partial(begin_kernel, 'sp'), out_shape=(jax.Shap...]
    unnamed x28 -> x24, local copies, waits for them, and re-layouts: 6.69 us -> 2.44 us
    ppermute x24 -> x27, waiting for transfers between devices: 21.1 us -> 24.7 us  [hop(): return lax.ppermute(value, 'sp', pairs)]
    pallas_call x2 -> x4, Pallas kernels: 9.28 us -> 7.2 us  [the longest x2 4.29 us: on_device(): pl.pallas_call(functools.partial(combine_kernel, places[low:high], 'sp'),...]
    ppermute x3 -> x4, waiting for transfers between devices: 27.2 us -> 28.1 us  [on_device(): pulled = lax.ppermute(parts[chunk], 'tp', swap)]
    ppermute x3 -> x4, starting transfers between devices: 3.58 us -> 4.18 us  [on_device(): pulled = lax.ppermute(parts[chunk], 'tp', swap)]
  transfers between devices with their start and end apart: 28 -> 32, of which waited for: 10 -> 13; matrix products, arithmetic and copies ran while one was open for 0% -> 0% of each run, Pallas kernels for 12% -> 15%
where the time goes in v2:
time: 102 us; the launch traced here: 101 us
  waiting for transfers between devices  54.4 us (53%)
  starting transfers between devices  27.3 us (27%)
  Pallas kernels  16.4 us (16%)
  local copies, waits for them, and re-layouts  2.44 us (2%)
    ppermute x4, waiting for transfers between devices, on_device(): pulled = lax.ppermute(parts[chunk], 'tp', swap)  28.1 us
    ppermute x27, waiting for transfers between devices, hop(): return lax.ppermute(value, 'sp', pairs)  24.7 us
    ppermute x27, starting transfers between devices, hop(): return lax.ppermute(value, 'sp', pairs)  21.7 us
    pallas_call x2, Pallas kernels, on_device(): pl.pallas_call(functools.partial(combine_kernel, places[low:high], 'sp'),...  4.29 us
    ppermute x4, starting transfers between devices, on_device(): pulled = lax.ppermute(parts[chunk], 'tp', swap)  4.18 us
    pallas_call x1, Pallas kernels, on_device(): pl.pallas_call(project_kernel, out_shape=jax.ShapeDtypeStruct((length, mo...  3.54 us
    pallas_call x4, Pallas kernels, attend(): pl.pallas_call(functools.partial(attend_kernel, stage, 'sp'), out_shape=(...  3.02 us
    pallas_call x1, Pallas kernels, on_device(): pl.pallas_call(functools.partial(cut_kernel, cuts, 'sp'), out_shape=[jax....  2.76 us
  transfers between devices with their start and end apart: 32, of which 13 were waited for; matrix products, arithmetic and copies ran while one was open for 0% of the time, Pallas kernels for 15%

profile of v2, /device:TPU:0, one launch (start us, length us, event | category | flops | bytes accessed | tf_op | source)
XLA Modules:
  0.0 101.3 jit_solution(6241224140576911863)
XLA Ops:
  2.9 5.2 %collective-permute-start = (bf16[288,512]{1,0:T(8,128)(2,1)S(1)}, bf16[288,512]{1,0:T(8,128)(2,1)S(1)}, u32[]{:S(2)}, u32[]{:S(2)}) collective-permute-start(bf16[288,512]{1,0:T(8,128)(2,1)S(1)} %pack.1.refs_7_), channel_id=1, source_target_pairs={{0,8},{2,10},{4,12},{6,14},{8,16},{10,18},{12,20},{14,22},{16,24},... | collective-permute-start | bytes 884744 | tf_op jit(solution)/shard_map/ppermute | solution.py:346
  8.1 3.4 %collective-permute-start.7 = (bf16[288,512]{1,0:T(8,128)(2,1)S(1)}, bf16[288,512]{1,0:T(8,128)(2,1)S(1)}, u32[]{:S(2)}, u32[]{:S(2)}) collective-permute-start(bf16[288,512]{1,0:T(8,128)(2,1)S(1)} %pack.1.refs_7_), channel_id=1, source_target_pairs={{0,4},{2,6},{8,12},{10,14},{16,20},{18,22},{24,28},{26,30},{1,5},{... | collective-permute-start | bytes 884744 | tf_op jit(solution)/shard_map/ppermute | solution.py:346
  11.6 2.8 %cut.1 = (bf16[1024,128]{1,0:T(8,128)(2,1)}, bf16[1024,256]{1,0:T(8,128)(2,1)}, bf16[1024,256]{1,0:T(8,128)(2,1)}, bf16[1024,256]{1,0:T(8,128)(2,1)}) custom-call(bf16[1024,4096]{1,0:T(8,128)(2,1)} %weight_hbm.1), custom_call_target="tpu_custom_call" | custom-call | flops 100000000 | bytes 10000000 | tf_op jit(solution)/shard_map/cut/pallas_call | solution.py:318
  14.3 1.6 %collective-permute-start.16 = (bf16[1024,128]{1,0:T(8,128)(2,1)}, bf16[1024,128]{1,0:T(8,128)(2,1)S(1)}, u32[]{:S(2)}, u32[]{:S(2)}) collective-permute-start(bf16[1024,128]{1,0:T(8,128)(2,1)} %get-tuple-element.34), channel_id=1, source_target_pairs={{0,1},{1,0},{2,3},{3,2},{4,5},{5,4},{6,7},{7,6},{8,9},{9,8},{10,11... | collective-permute-start | bytes 786440 | tf_op jit(solution)/shard_map/ppermute | solution.py:372
  16.4 7.4 %collective-permute-done.16.refs_0_ = bf16[1024,128]{1,0:T(8,128)(2,1)S(1)} collective-permute-done((bf16[1024,128]{1,0:T(8,128)(2,1)}, bf16[1024,128]{1,0:T(8,128)(2,1)S(1)}, u32[]{:S(2)}, u32[]{:S(2)}) %collective-permute-start.16) | collective-permute-done | bytes 262176 | tf_op jit(solution)/shard_map/ppermute | solution.py:372
  23.8 1.6 %collective-permute-start.18 = (bf16[1024,128]{1,0:T(8,128)(2,1)S(1)}, bf16[1024,128]{1,0:T(8,128)(2,1)S(1)}, u32[]{:S(2)}, u32[]{:S(2)}) collective-permute-start(bf16[1024,128]{1,0:T(8,128)(2,1)S(1)} %collective-permute-done.16.refs_0_), channel_id=1, source_target_pairs={{0,8},{2,10},{4,12},{6,14},{8,0},{10,2},{12,4},{14,6},{16,24},{18,... | collective-permute-start | bytes 786440 | tf_op jit(solution)/shard_map/ppermute | solution.py:346
  25.4 1.5 %collective-permute-start.28 = (bf16[1024,256]{1,0:T(8,128)(2,1)}, bf16[1024,256]{1,0:T(8,128)(2,1)S(1)}, u32[]{:S(2)}, u32[]{:S(2)}) collective-permute-start(bf16[1024,256]{1,0:T(8,128)(2,1)} %get-tuple-element.36), channel_id=1, source_target_pairs={{0,1},{1,0},{2,3},{3,2},{4,5},{5,4},{6,7},{7,6},{8,9},{9,8},{10,11... | collective-permute-start | bytes 1572872 | tf_op jit(solution)/shard_map/ppermute | solution.py:372
  27.5 2.7 %collective-permute-done.18.refs_2_ = bf16[1024,128]{1,0:T(8,128)(2,1)S(1)} collective-permute-done((bf16[1024,128]{1,0:T(8,128)(2,1)S(1)}, bf16[1024,128]{1,0:T(8,128)(2,1)S(1)}, u32[]{:S(2)}, u32[]{:S(2)}) %collective-permute-start.18) | collective-permute-done | bytes 262176 | tf_op jit(solution)/shard_map/ppermute | solution.py:346
  30.8 2.4 %collective-permute-done.20.refs_4_ = bf16[1024,128]{1,0:T(8,128)(2,1)S(1)} collective-permute-done((bf16[1024,128]{1,0:T(8,128)(2,1)S(1)}, bf16[1024,128]{1,0:T(8,128)(2,1)S(1)}, u32[]{:S(2)}, u32[]{:S(2)}) %collective-permute-start.20) | collective-permute-done | bytes 262176 | tf_op jit(solution)/shard_map/ppermute | solution.py:346
  33.2 1.8 %collective-permute-done.24.refs_8_ = bf16[1024,256]{1,0:T(8,128)(2,1)S(1)} collective-permute-done((bf16[1024,256]{1,0:T(8,128)(2,1)}, bf16[1024,256]{1,0:T(8,128)(2,1)S(1)}, u32[]{:S(2)}, u32[]{:S(2)}) %collective-permute-start.24) | collective-permute-done | bytes 524320 | tf_op jit(solution)/shard_map/ppermute | solution.py:372
  35.0 11.2 %collective-permute-done.28.refs_12_ = bf16[1024,256]{1,0:T(8,128)(2,1)S(1)} collective-permute-done((bf16[1024,256]{1,0:T(8,128)(2,1)}, bf16[1024,256]{1,0:T(8,128)(2,1)S(1)}, u32[]{:S(2)}, u32[]{:S(2)}) %collective-permute-start.28) | collective-permute-done | bytes 524320 | tf_op jit(solution)/shard_map/ppermute | solution.py:372
  48.1 7.7 %collective-permute-done.12.refs_0_ = bf16[1024,256]{1,0:T(8,128)(2,1)S(1)} collective-permute-done((bf16[1024,256]{1,0:T(8,128)(2,1)}, bf16[1024,256]{1,0:T(8,128)(2,1)S(1)}, u32[]{:S(2)}, u32[]{:S(2)}) %collective-permute-start.12) | collective-permute-done | bytes 524320 | tf_op jit(solution)/shard_map/ppermute | solution.py:372
  56.4 2.0 %collective-permute-done.2.refs_5_ = bf16[288,512]{1,0:T(8,128)(2,1)S(1)} collective-permute-done((bf16[288,512]{1,0:T(8,128)(2,1)S(1)}, bf16[288,512]{1,0:T(8,128)(2,1)S(1)}, u32[]{:S(2)}, u32[]{:S(2)}) %collective-permute-start.2) | collective-permute-done | bytes 294944 | tf_op jit(solution)/shard_map/ppermute | solution.py:346
  58.4 2.4 %begin.1 = (bf16[8,256,256]{2,1,0:T(8,128)(2,1)S(1)}, bf16[1024,512]{1,0:T(8,128)(2,1)S(1)}, f32[16,256]{1,0:T(8,128)S(1)}, f32[8,128,256]{2,1,0:T(8,128)S(1)}) custom-call(bf16[256,1024]{1,0:T(8,128)(2,1)S(1)} %copy-done.4, f32[1,1024]{1,0:T(1,128)S(1)} %bitcast.7, bf16[1024,1024]{1,0:T(8,128)(2,1)S(1)} %copy-done, bf16[1024,512]{1,0:T(8,128)(2,1)S(1)} %copy-done.1, ...), custom_call_target="tpu_custom_call" | custom-call | flops 2000000000 | bytes 6000000 | tf_op jit(solution)/shard_map/begin/pallas_call | solution.py:386
  60.9 2.3 %collective-permute-done.22.refs_6_ = bf16[1024,128]{1,0:T(8,128)(2,1)S(1)} collective-permute-done((bf16[1024,128]{1,0:T(8,128)(2,1)S(1)}, bf16[1024,128]{1,0:T(8,128)(2,1)S(1)}, u32[]{:S(2)}, u32[]{:S(2)}) %collective-permute-start.22) | collective-permute-done | bytes 262176 | tf_op jit(solution)/shard_map/ppermute | solution.py:346
  64.7 2.7 %collective-permute-start.26 = (bf16[1024,256]{1,0:T(8,128)(2,1)S(1)}, bf16[1024,256]{1,0:T(8,128)(2,1)S(1)}, u32[]{:S(2)}, u32[]{:S(2)}) collective-permute-start(bf16[1024,256]{1,0:T(8,128)(2,1)S(1)} %collective-permute-done.24.refs_8_), channel_id=1, source_target_pairs={{0,8},{2,10},{4,12},{6,14},{8,0},{10,2},{12,4},{14,6},{16,24},{18,... | collective-permute-start | bytes 1572872 | tf_op jit(solution)/shard_map/ppermute | solution.py:346
  72.6 7.0 %collective-permute-done.26.refs_10_ = bf16[1024,256]{1,0:T(8,128)(2,1)S(1)} collective-permute-done((bf16[1024,256]{1,0:T(8,128)(2,1)S(1)}, bf16[1024,256]{1,0:T(8,128)(2,1)S(1)}, u32[]{:S(2)}, u32[]{:S(2)}) %collective-permute-start.26) | collective-permute-done | bytes 524320 | tf_op jit(solution)/shard_map/ppermute | solution.py:346
  79.5 1.5 %collective-permute-start.27 = (bf16[1024,256]{1,0:T(8,128)(2,1)S(1)}, bf16[1024,256]{1,0:T(8,128)(2,1)S(1)}, u32[]{:S(2)}, u32[]{:S(2)}) collective-permute-start(bf16[1024,256]{1,0:T(8,128)(2,1)S(1)} %collective-permute-done.26.refs_10_), channel_id=1, source_target_pairs={{0,2},{2,0},{4,6},{6,4},{8,10},{10,8},{12,14},{14,12},{16,18},{18,... | collective-permute-start | bytes 1572872 | tf_op jit(solution)/shard_map/ppermute | solution.py:346
  82.5 1.5 %collective-permute-start.11 = (bf16[256,1024]{1,0:T(8,128)(2,1)S(1)}, bf16[256,1024]{1,0:T(8,128)(2,1)S(1)}, u32[]{:S(2)}, u32[]{:S(2)}) collective-permute-start(bf16[256,1024]{1,0:T(8,128)(2,1)S(1)} %finish.1.rows_ref), channel_id=1, source_target_pairs={{0,1},{1,0},{2,3},{3,2},{4,5},{5,4},{6,7},{7,6},{8,9},{9,8},{10,11... | collective-permute-start | bytes 1572872 | tf_op jit(solution)/shard_map/ppermute | solution.py:444
  84.2 6.5 %collective-permute-done.14.refs_2_ = bf16[1024,256]{1,0:T(8,128)(2,1)S(1)} collective-permute-done((bf16[1024,256]{1,0:T(8,128)(2,1)S(1)}, bf16[1024,256]{1,0:T(8,128)(2,1)S(1)}, u32[]{:S(2)}, u32[]{:S(2)}) %collective-permute-start.14) | collective-permute-done | bytes 524320 | tf_op jit(solution)/shard_map/ppermute | solution.py:346
  91.6 3.5 %ours.1.ours_ref = bf16[256,4096]{1,0:T(8,128)(2,1)S(1)} custom-call(bf16[256,1024]{1,0:T(8,128)(2,1)S(1)} %finish.1.rows_ref, bf16[1024,4096]{1,0:T(8,128)(2,1)S(1)} %bitcast.5), custom_call_target="tpu_custom_call" | custom-call | flops 2000000000 | bytes 10000000 | tf_op jit(solution)/shard_map/ours/pallas_call | solution.py:445
  95.2 1.7 %collective-permute-done.11.rows_ref = bf16[256,1024]{1,0:T(8,128)(2,1)S(1)} collective-permute-done((bf16[256,1024]{1,0:T(8,128)(2,1)S(1)}, bf16[256,1024]{1,0:T(8,128)(2,1)S(1)}, u32[]{:S(2)}, u32[]{:S(2)}) %collective-permute-start.11) | collective-permute-done | bytes 524320 | tf_op jit(solution)/shard_map/ppermute | solution.py:444
  96.9 2.8 %shard_map.113.refs_4_ = bf16[256,4096]{1,0:T(8,128)(2,1)} custom-call(bf16[256,1024]{1,0:T(8,128)(2,1)S(1)} %collective-permute-done.11.rows_ref, bf16[256,4096]{1,0:T(8,128)(2,1)S(1)} %ours.1.ours_ref, bf16[1024,128]{1,0:T(8,128)(2,1)S(1)} %collective-permute-done.16.refs_0_, bf16[1024,128]{1,0:T(8,128)(2,1)S(1)} %collective-permute-done.17.refs_1_, ...), custom_call_target="tpu_custom_call" | custom-call | flops 1000000000 | bytes 5000000 | tf_op jit(solution)/shard_map/pallas_call | solution.py:463
  99.7 1.5 %shard_map.114 = bf16[256,4096]{1,0:T(8,128)(2,1)} custom-call(bf16[256,1024]{1,0:T(8,128)(2,1)S(1)} %collective-permute-done.11.rows_ref, bf16[256,4096]{1,0:T(8,128)(2,1)S(1)} %ours.1.ours_ref, bf16[1024,256]{1,0:T(8,128)(2,1)S(1)} %collective-permute-done.12.refs_0_, ...), custom_call_target="tpu_custom_call", output_to_operand_aliasing={{}: (6, {})} | custom-call | flops 1000000000 | bytes 5000000 | tf_op jit(solution)/shard_map/pallas_call | solution.py:463
  (79 shorter events, 16.1 us)
Async XLA Ops:
  2.9 22.5 %collective-permute-start = (bf16[288,512]{1,0:T(8,128)(2,1)S(1)}, bf16[288,512]{1,0:T(8,128)(2,1)S(1)}, u32[]{:S(2)}, u32[]{:S(2)}) collective-permute-start(bf16[288,512]{1,0:T(8,128)(2,1)S(1)} %pack.1.refs_7_), channel_id=1, source_target_pairs={{0,8},{2,10},{4,12},{6,14},{8,16},{10,18},{12,20},{14,22},{16,24},... | collective-permute-start | bytes 884744 | tf_op jit(solution)/shard_map/ppermute | solution.py:346
  8.1 18.7 %collective-permute-start.7 = (bf16[288,512]{1,0:T(8,128)(2,1)S(1)}, bf16[288,512]{1,0:T(8,128)(2,1)S(1)}, u32[]{:S(2)}, u32[]{:S(2)}) collective-permute-start(bf16[288,512]{1,0:T(8,128)(2,1)S(1)} %pack.1.refs_7_), channel_id=1, source_target_pairs={{0,4},{2,6},{8,12},{10,14},{16,20},{18,22},{24,28},{26,30},{1,5},{... | collective-permute-start | bytes 884744 | tf_op jit(solution)/shard_map/ppermute | solution.py:346
  15.9 11.0 %collective-permute-start.10 = (bf16[288,512]{1,0:T(8,128)(2,1)S(1)}, bf16[288,512]{1,0:T(8,128)(2,1)S(1)}, u32[]{:S(2)}, u32[]{:S(2)}) collective-permute-start(bf16[288,512]{1,0:T(8,128)(2,1)S(1)} %pack.1.refs_7_), channel_id=1, source_target_pairs={{0,2},{2,0},{4,6},{6,4},{8,10},{10,8},{12,14},{14,12},{16,18},{18,... | collective-permute-start | bytes 884744 | tf_op jit(solution)/shard_map/ppermute | solution.py:346
  15.9 19.1 %collective-permute-start.24 = (bf16[1024,256]{1,0:T(8,128)(2,1)}, bf16[1024,256]{1,0:T(8,128)(2,1)S(1)}, u32[]{:S(2)}, u32[]{:S(2)}) collective-permute-start(bf16[1024,256]{1,0:T(8,128)(2,1)} %get-tuple-element.35), channel_id=1, source_target_pairs={{0,1},{1,0},{2,3},{3,2},{4,5},{5,4},{6,7},{7,6},{8,9},{9,8},{10,11... | collective-permute-start | bytes 1572872 | tf_op jit(solution)/shard_map/ppermute | solution.py:372
  25.4 20.9 %collective-permute-start.28 = (bf16[1024,256]{1,0:T(8,128)(2,1)}, bf16[1024,256]{1,0:T(8,128)(2,1)S(1)}, u32[]{:S(2)}, u32[]{:S(2)}) collective-permute-start(bf16[1024,256]{1,0:T(8,128)(2,1)} %get-tuple-element.36), channel_id=1, source_target_pairs={{0,1},{1,0},{2,3},{3,2},{4,5},{5,4},{6,7},{7,6},{8,9},{9,8},{10,11... | collective-permute-start | bytes 1572872 | tf_op jit(solution)/shard_map/ppermute | solution.py:372
  26.9 28.9 %collective-permute-start.12 = (bf16[1024,256]{1,0:T(8,128)(2,1)}, bf16[1024,256]{1,0:T(8,128)(2,1)S(1)}, u32[]{:S(2)}, u32[]{:S(2)}) collective-permute-start(bf16[1024,256]{1,0:T(8,128)(2,1)} %get-tuple-element.33), channel_id=1, source_target_pairs={{0,1},{1,0},{2,3},{3,2},{4,5},{5,4},{6,7},{7,6},{8,9},{9,8},{10,11... | collective-permute-start | bytes 1572872 | tf_op jit(solution)/shard_map/ppermute | solution.py:372
  30.2 16.6 %collective-permute-start.1 = (bf16[288,512]{1,0:T(8,128)(2,1)S(1)}, bf16[288,512]{1,0:T(8,128)(2,1)S(1)}, u32[]{:S(2)}, u32[]{:S(2)}) collective-permute-start(bf16[288,512]{1,0:T(8,128)(2,1)S(1)} %collective-permute-done.refs_7_), channel_id=1, source_target_pairs={{2,10},{4,12},{6,14},{10,18},{12,20},{14,22},{18,26},{20,28},{22,3... | collective-permute-start | bytes 884744 | tf_op jit(solution)/shard_map/ppermute | solution.py:346
  33.2 13.0 %collective-permute-start.17 = (bf16[1024,128]{1,0:T(8,128)(2,1)S(1)}, bf16[1024,128]{1,0:T(8,128)(2,1)S(1)}, u32[]{:S(2)}, u32[]{:S(2)}) collective-permute-start(bf16[1024,128]{1,0:T(8,128)(2,1)S(1)} %collective-permute-done.16.refs_0_), channel_id=1, source_target_pairs={{0,2},{2,0},{4,6},{6,4},{8,10},{10,8},{12,14},{14,12},{16,18},{18,... | collective-permute-start | bytes 786440 | tf_op jit(solution)/shard_map/ppermute | solution.py:346
  35.0 20.8 %collective-permute-start.4 = (bf16[288,512]{1,0:T(8,128)(2,1)S(1)}, bf16[288,512]{1,0:T(8,128)(2,1)S(1)}, u32[]{:S(2)}, u32[]{:S(2)}) collective-permute-start(bf16[288,512]{1,0:T(8,128)(2,1)S(1)} %collective-permute-done.refs_7_), channel_id=1, source_target_pairs={{0,4},{2,6},{4,0},{6,2},{8,12},{10,14},{12,8},{14,10},{16,20},{18,... | collective-permute-start | bytes 884744 | tf_op jit(solution)/shard_map/ppermute | solution.py:346
  46.3 9.6 %collective-permute-start.9 = (bf16[288,512]{1,0:T(8,128)(2,1)S(1)}, bf16[288,512]{1,0:T(8,128)(2,1)S(1)}, u32[]{:S(2)}, u32[]{:S(2)}) collective-permute-start(bf16[288,512]{1,0:T(8,128)(2,1)S(1)} %collective-permute-done.refs_7_), channel_id=1, source_target_pairs={{0,2},{2,0},{4,6},{6,4},{8,10},{10,8},{12,14},{14,12},{16,18},{18,... | collective-permute-start | bytes 884744 | tf_op jit(solution)/shard_map/ppermute | solution.py:346
  46.3 10.1 %collective-permute-start.8 = (bf16[288,512]{1,0:T(8,128)(2,1)S(1)}, bf16[288,512]{1,0:T(8,128)(2,1)S(1)}, u32[]{:S(2)}, u32[]{:S(2)}) collective-permute-start(bf16[288,512]{1,0:T(8,128)(2,1)S(1)} %collective-permute-done.7.refs_6_), channel_id=1, source_target_pairs={{0,2},{2,0},{4,6},{6,4},{8,10},{10,8},{12,14},{14,12},{16,18},{18,... | collective-permute-start | bytes 884744 | tf_op jit(solution)/shard_map/ppermute | solution.py:346
  46.8 11.6 %collective-permute-start.2 = (bf16[288,512]{1,0:T(8,128)(2,1)S(1)}, bf16[288,512]{1,0:T(8,128)(2,1)S(1)}, u32[]{:S(2)}, u32[]{:S(2)}) collective-permute-start(bf16[288,512]{1,0:T(8,128)(2,1)S(1)} %collective-permute-done.1), channel_id=1, source_target_pairs={{4,0},{6,2},{12,8},{14,10},{20,16},{22,18},{28,24},{30,26},{5,1},{... | collective-permute-start | bytes 884744 | tf_op jit(solution)/shard_map/ppermute | solution.py:346
  55.8 12.8 %collective-permute-start.6 = (bf16[288,512]{1,0:T(8,128)(2,1)S(1)}, bf16[288,512]{1,0:T(8,128)(2,1)S(1)}, u32[]{:S(2)}, u32[]{:S(2)}) collective-permute-start(bf16[288,512]{1,0:T(8,128)(2,1)S(1)} %collective-permute-done.1), channel_id=1, source_target_pairs={{0,2},{2,0},{4,6},{6,4},{8,10},{10,8},{12,14},{14,12},{16,18},{18,... | collective-permute-start | bytes 884744 | tf_op jit(solution)/shard_map/ppermute | solution.py:346
  56.3 11.2 %collective-permute-start.5 = (bf16[288,512]{1,0:T(8,128)(2,1)S(1)}, bf16[288,512]{1,0:T(8,128)(2,1)S(1)}, u32[]{:S(2)}, u32[]{:S(2)}) collective-permute-start(bf16[288,512]{1,0:T(8,128)(2,1)S(1)} %collective-permute-done.4.refs_7_), channel_id=1, source_target_pairs={{0,2},{2,0},{4,6},{6,4},{8,10},{10,8},{12,14},{14,12},{16,18},{18,... | collective-permute-start | bytes 884744 | tf_op jit(solution)/shard_map/ppermute | solution.py:346
  58.4 11.2 %collective-permute-start.3 = (bf16[288,512]{1,0:T(8,128)(2,1)S(1)}, bf16[288,512]{1,0:T(8,128)(2,1)S(1)}, u32[]{:S(2)}, u32[]{:S(2)}) collective-permute-start(bf16[288,512]{1,0:T(8,128)(2,1)S(1)} %collective-permute-done.2.refs_5_), channel_id=1, source_target_pairs={{0,2},{2,0},{4,6},{6,4},{8,10},{10,8},{12,14},{14,12},{16,18},{18,... | collective-permute-start | bytes 884744 | tf_op jit(solution)/shard_map/ppermute | solution.py:346
  64.7 14.8 %collective-permute-start.26 = (bf16[1024,256]{1,0:T(8,128)(2,1)S(1)}, bf16[1024,256]{1,0:T(8,128)(2,1)S(1)}, u32[]{:S(2)}, u32[]{:S(2)}) collective-permute-start(bf16[1024,256]{1,0:T(8,128)(2,1)S(1)} %collective-permute-done.24.refs_8_), channel_id=1, source_target_pairs={{0,8},{2,10},{4,12},{6,14},{8,0},{10,2},{12,4},{14,6},{16,24},{18,... | collective-permute-start | bytes 1572872 | tf_op jit(solution)/shard_map/ppermute | solution.py:346
  67.5 15.0 %collective-permute-start.25 = (bf16[1024,256]{1,0:T(8,128)(2,1)S(1)}, bf16[1024,256]{1,0:T(8,128)(2,1)S(1)}, u32[]{:S(2)}, u32[]{:S(2)}) collective-permute-start(bf16[1024,256]{1,0:T(8,128)(2,1)S(1)} %collective-permute-done.24.refs_8_), channel_id=1, source_target_pairs={{0,2},{2,0},{4,6},{6,4},{8,10},{10,8},{12,14},{14,12},{16,18},{18,... | collective-permute-start | bytes 1572872 | tf_op jit(solution)/shard_map/ppermute | solution.py:346
  68.6 13.9 %collective-permute-start.30 = (bf16[1024,256]{1,0:T(8,128)(2,1)S(1)}, bf16[1024,256]{1,0:T(8,128)(2,1)S(1)}, u32[]{:S(2)}, u32[]{:S(2)}) collective-permute-start(bf16[1024,256]{1,0:T(8,128)(2,1)S(1)} %collective-permute-done.28.refs_12_), channel_id=1, source_target_pairs={{0,4},{2,6},{4,0},{6,2},{8,12},{10,14},{12,8},{14,10},{16,20},{18,... | collective-permute-start | bytes 1572872 | tf_op jit(solution)/shard_map/ppermute | solution.py:346
  69.6 14.5 %collective-permute-start.29 = (bf16[1024,256]{1,0:T(8,128)(2,1)S(1)}, bf16[1024,256]{1,0:T(8,128)(2,1)S(1)}, u32[]{:S(2)}, u32[]{:S(2)}) collective-permute-start(bf16[1024,256]{1,0:T(8,128)(2,1)S(1)} %collective-permute-done.28.refs_12_), channel_id=1, source_target_pairs={{0,2},{2,0},{4,6},{6,4},{8,10},{10,8},{12,14},{14,12},{16,18},{18,... | collective-permute-start | bytes 1572872 | tf_op jit(solution)/shard_map/ppermute | solution.py:346
  69.6 21.2 %collective-permute-start.14 = (bf16[1024,256]{1,0:T(8,128)(2,1)S(1)}, bf16[1024,256]{1,0:T(8,128)(2,1)S(1)}, u32[]{:S(2)}, u32[]{:S(2)}) collective-permute-start(bf16[1024,256]{1,0:T(8,128)(2,1)S(1)} %collective-permute-done.12.refs_0_), channel_id=1, source_target_pairs={{0,8},{2,10},{4,12},{6,14},{8,0},{10,2},{12,4},{14,6},{16,24},{18,... | collective-permute-start | bytes 1572872 | tf_op jit(solution)/shard_map/ppermute | solution.py:346
  79.5 15.6 %collective-permute-start.27 = (bf16[1024,256]{1,0:T(8,128)(2,1)S(1)}, bf16[1024,256]{1,0:T(8,128)(2,1)S(1)}, u32[]{:S(2)}, u32[]{:S(2)}) collective-permute-start(bf16[1024,256]{1,0:T(8,128)(2,1)S(1)} %collective-permute-done.26.refs_10_), channel_id=1, source_target_pairs={{0,2},{2,0},{4,6},{6,4},{8,10},{10,8},{12,14},{14,12},{16,18},{18,... | collective-permute-start | bytes 1572872 | tf_op jit(solution)/shard_map/ppermute | solution.py:346
  82.5 12.7 %collective-permute-start.31 = (bf16[1024,256]{1,0:T(8,128)(2,1)S(1)}, bf16[1024,256]{1,0:T(8,128)(2,1)S(1)}, u32[]{:S(2)}, u32[]{:S(2)}) collective-permute-start(bf16[1024,256]{1,0:T(8,128)(2,1)S(1)} %collective-permute-done.30.refs_14_), channel_id=1, source_target_pairs={{0,2},{2,0},{4,6},{6,4},{8,10},{10,8},{12,14},{14,12},{16,18},{18,... | collective-permute-start | bytes 1572872 | tf_op jit(solution)/shard_map/ppermute | solution.py:346
  82.5 14.3 %collective-permute-start.11 = (bf16[256,1024]{1,0:T(8,128)(2,1)S(1)}, bf16[256,1024]{1,0:T(8,128)(2,1)S(1)}, u32[]{:S(2)}, u32[]{:S(2)}) collective-permute-start(bf16[256,1024]{1,0:T(8,128)(2,1)S(1)} %finish.1.rows_ref), channel_id=1, source_target_pairs={{0,1},{1,0},{2,3},{3,2},{4,5},{5,4},{6,7},{7,6},{8,9},{9,8},{10,11... | collective-permute-start | bytes 1572872 | tf_op jit(solution)/shard_map/ppermute | solution.py:444
  84.0 15.7 %collective-permute-start.13 = (bf16[1024,256]{1,0:T(8,128)(2,1)S(1)}, bf16[1024,256]{1,0:T(8,128)(2,1)S(1)}, u32[]{:S(2)}, u32[]{:S(2)}) collective-permute-start(bf16[1024,256]{1,0:T(8,128)(2,1)S(1)} %collective-permute-done.12.refs_0_), channel_id=1, source_target_pairs={{0,2},{2,0},{4,6},{6,4},{8,10},{10,8},{12,14},{14,12},{16,18},{18,... | collective-permute-start | bytes 1572872 | tf_op jit(solution)/shard_map/ppermute | solution.py:346
  (20 other events, 485.9 us)

commit v3 on v2

--- a/solution.py
+++ b/solution.py
@@ -11,8 +11,7 @@
 ROTARY = 64
 VALUE_DIM = 128
 GROUP = 4
-KINDS = (("quad", 1), ("z", 2), ("y", 2), ("z", 2))
-EARLY = 16
+KINDS = (("quad", 1), ("z", 2), ("y", 2), ("z", 1), ("z", 1))
 
 norm_eps = 1e-06
 rope_theta = 10000.0
@@ -454,7 +453,7 @@
         name="ours",
     )(attended, output_weight)
     mixed = None
-    for low, high in ((0, EARLY), (EARLY, len(pieces))):
+    for low, high in ((0, len(pieces)),):
         operands = [theirs, ours, *pieces[low:high]]
         aliases = {}
         if mixed is not None:

time: 102 us -> 109 us (1.069)
  starting transfers between devices: 27.3 us -> 43.5 us
  waiting for transfers between devices: 54.4 us -> 48.4 us
  local copies, waits for them, and re-layouts: 2.44 us -> 0.08 us
    ppermute x4 -> x5, waiting for transfers between devices: 28.1 us -> 14.3 us  [on_device(): pulled = lax.ppermute(parts[chunk], 'tp', swap)]
    ppermute x27 -> x30, starting transfers between devices: 21.7 us -> 34.3 us  [hop(): return lax.ppermute(value, 'sp', pairs)]
    ppermute x1, waiting for transfers between devices: 1.67 us -> 9.12 us  [on_device(): theirs = lax.ppermute(attended, 'tp', swap)]
    ppermute x4 -> x5, starting transfers between devices: 4.18 us -> 7.7 us  [on_device(): pulled = lax.ppermute(parts[chunk], 'tp', swap)]
    unnamed x24 -> x28, local copies, waits for them, and re-layouts: 2.44 us -> 0.08 us
    pallas_call x2 -> x1, Pallas kernels: 4.29 us -> 3.51 us  [on_device(): pl.pallas_call(functools.partial(combine_kernel, places[low:high], 'sp'),...]
    ppermute x27 -> x30, waiting for transfers between devices: 24.7 us -> 25 us  [hop(): return lax.ppermute(value, 'sp', pairs)]
  transfers between devices with their start and end apart: 32 -> 36, of which waited for: 13 -> 10; matrix products, arithmetic and copies ran while one was open for 0% -> 0% of each run, Pallas kernels for 15% -> 9%
where the time goes in v3:
time: 109 us; the launch traced here: 108 us
  waiting for transfers between devices  48.4 us (44%)
  starting transfers between devices  43.5 us (40%)
  Pallas kernels  15.7 us (14%)
    ppermute x30, starting transfers between devices, hop(): return lax.ppermute(value, 'sp', pairs)  34.3 us
    ppermute x30, waiting for transfers between devices, hop(): return lax.ppermute(value, 'sp', pairs)  25 us
    ppermute x5, waiting for transfers between devices, on_device(): pulled = lax.ppermute(parts[chunk], 'tp', swap)  14.3 us
    ppermute x1, waiting for transfers between devices, on_device(): theirs = lax.ppermute(attended, 'tp', swap)  9.12 us
    ppermute x5, starting transfers between devices, on_device(): pulled = lax.ppermute(parts[chunk], 'tp', swap)  7.7 us
    pallas_call x1, Pallas kernels, on_device(): pl.pallas_call(project_kernel, out_shape=jax.ShapeDtypeStruct((length, mo...  3.54 us
    pallas_call x1, Pallas kernels, on_device(): pl.pallas_call(functools.partial(combine_kernel, places[low:high], 'sp'),...  3.51 us
    pallas_call x4, Pallas kernels, attend(): pl.pallas_call(functools.partial(attend_kernel, stage, 'sp'), out_shape=(...  3.01 us
  transfers between devices with their start and end apart: 36, of which 10 were waited for; matrix products, arithmetic and copies ran while one was open for 0% of the time, Pallas kernels for 9%

profile of v3, /device:TPU:0, one launch (start us, length us, event | category | flops | bytes accessed | tf_op | source)
XLA Modules:
  0.0 108.5 jit_solution(15393991063253560690)
XLA Ops:
  0.0 2.8 %cut.1 = (bf16[1024,128]{1,0:T(8,128)(2,1)}, bf16[1024,256]{1,0:T(8,128)(2,1)}, bf16[1024,256]{1,0:T(8,128)(2,1)}, bf16[1024,128]{1,0:T(8,128)(2,1)}, bf16[1024,128]{1,0:T(8,128)(2,1)}) custom-call(bf16[1024,4096]{1,0:T(8,128)(2,1)} %weight_hbm.1), custom_call_target="tpu_custom_call" | custom-call | flops 100000000 | bytes 10000000 | tf_op jit(solution)/shard_map/cut/pallas_call | solution.py:317
  2.8 3.0 %collective-permute-start.12 = (bf16[1024,128]{1,0:T(8,128)(2,1)}, bf16[1024,128]{1,0:T(8,128)(2,1)S(1)}, u32[]{:S(2)}, u32[]{:S(2)}) collective-permute-start(bf16[1024,128]{1,0:T(8,128)(2,1)} %get-tuple-element.34), channel_id=1, source_target_pairs={{0,1},{1,0},{2,3},{3,2},{4,5},{5,4},{6,7},{7,6},{8,9},{9,8},{10,11... | collective-permute-start | bytes 786440 | tf_op jit(solution)/shard_map/ppermute | solution.py:371
  5.9 1.9 %collective-permute-start.32 = (bf16[1024,128]{1,0:T(8,128)(2,1)}, bf16[1024,128]{1,0:T(8,128)(2,1)S(1)}, u32[]{:S(2)}, u32[]{:S(2)}) collective-permute-start(bf16[1024,128]{1,0:T(8,128)(2,1)} %get-tuple-element.38), channel_id=1, source_target_pairs={{0,1},{1,0},{2,3},{3,2},{4,5},{5,4},{6,7},{7,6},{8,9},{9,8},{10,11... | collective-permute-start | bytes 786440 | tf_op jit(solution)/shard_map/ppermute | solution.py:371
  8.4 3.8 %collective-permute-start = (bf16[288,512]{1,0:T(8,128)(2,1)S(1)}, bf16[288,512]{1,0:T(8,128)(2,1)S(1)}, u32[]{:S(2)}, u32[]{:S(2)}) collective-permute-start(bf16[288,512]{1,0:T(8,128)(2,1)S(1)} %pack.1.refs_7_), channel_id=1, source_target_pairs={{0,8},{2,10},{4,12},{6,14},{8,16},{10,18},{12,20},{14,22},{16,24},... | collective-permute-start | bytes 884744 | tf_op jit(solution)/shard_map/ppermute | solution.py:345
  12.2 3.4 %collective-permute-start.7 = (bf16[288,512]{1,0:T(8,128)(2,1)S(1)}, bf16[288,512]{1,0:T(8,128)(2,1)S(1)}, u32[]{:S(2)}, u32[]{:S(2)}) collective-permute-start(bf16[288,512]{1,0:T(8,128)(2,1)S(1)} %pack.1.refs_7_), channel_id=1, source_target_pairs={{0,4},{2,6},{8,12},{10,14},{16,20},{18,22},{24,28},{26,30},{1,5},{... | collective-permute-start | bytes 884744 | tf_op jit(solution)/shard_map/ppermute | solution.py:345
  16.2 2.6 %collective-permute-done.28.refs_16_ = bf16[1024,128]{1,0:T(8,128)(2,1)S(1)} collective-permute-done((bf16[1024,128]{1,0:T(8,128)(2,1)}, bf16[1024,128]{1,0:T(8,128)(2,1)S(1)}, u32[]{:S(2)}, u32[]{:S(2)}) %collective-permute-start.28) | collective-permute-done | bytes 262176 | tf_op jit(solution)/shard_map/ppermute | solution.py:371
  18.8 2.0 %collective-permute-start.24 = (bf16[1024,256]{1,0:T(8,128)(2,1)S(1)}, bf16[1024,256]{1,0:T(8,128)(2,1)S(1)}, u32[]{:S(2)}, u32[]{:S(2)}) collective-permute-start(bf16[1024,256]{1,0:T(8,128)(2,1)S(1)} %copy-done.10), channel_id=1, source_target_pairs={{0,1},{1,0},{2,3},{3,2},{4,5},{5,4},{6,7},{7,6},{8,9},{9,8},{10,11... | collective-permute-start | bytes 1572872 | tf_op jit(solution)/shard_map/ppermute | solution.py:371
  20.9 3.6 %collective-permute-done.32.refs_20_ = bf16[1024,128]{1,0:T(8,128)(2,1)S(1)} collective-permute-done((bf16[1024,128]{1,0:T(8,128)(2,1)}, bf16[1024,128]{1,0:T(8,128)(2,1)S(1)}, u32[]{:S(2)}, u32[]{:S(2)}) %collective-permute-start.32) | collective-permute-done | bytes 262176 | tf_op jit(solution)/shard_map/ppermute | solution.py:371
  24.5 2.1 %collective-permute-start.14 = (bf16[1024,128]{1,0:T(8,128)(2,1)S(1)}, bf16[1024,128]{1,0:T(8,128)(2,1)S(1)}, u32[]{:S(2)}, u32[]{:S(2)}) collective-permute-start(bf16[1024,128]{1,0:T(8,128)(2,1)S(1)} %collective-permute-done.12.refs_0_), channel_id=1, source_target_pairs={{0,8},{2,10},{4,12},{6,14},{8,0},{10,2},{12,4},{14,6},{16,24},{18,... | collective-permute-start | bytes 786440 | tf_op jit(solution)/shard_map/ppermute | solution.py:345
  26.6 1.5 %collective-permute-start.16 = (bf16[1024,128]{1,0:T(8,128)(2,1)S(1)}, bf16[1024,128]{1,0:T(8,128)(2,1)S(1)}, u32[]{:S(2)}, u32[]{:S(2)}) collective-permute-start(bf16[1024,128]{1,0:T(8,128)(2,1)S(1)} %collective-permute-done.12.refs_0_), channel_id=1, source_target_pairs={{0,4},{2,6},{4,0},{6,2},{8,12},{10,14},{12,8},{14,10},{16,20},{18,... | collective-permute-start | bytes 786440 | tf_op jit(solution)/shard_map/ppermute | solution.py:345
  28.5 5.2 %collective-permute-done.14.refs_2_ = bf16[1024,128]{1,0:T(8,128)(2,1)S(1)} collective-permute-done((bf16[1024,128]{1,0:T(8,128)(2,1)S(1)}, bf16[1024,128]{1,0:T(8,128)(2,1)S(1)}, u32[]{:S(2)}, u32[]{:S(2)}) %collective-permute-start.14) | collective-permute-done | bytes 262176 | tf_op jit(solution)/shard_map/ppermute | solution.py:345
  35.0 1.5 %collective-permute-start.34 = (bf16[1024,128]{1,0:T(8,128)(2,1)S(1)}, bf16[1024,128]{1,0:T(8,128)(2,1)S(1)}, u32[]{:S(2)}, u32[]{:S(2)}) collective-permute-start(bf16[1024,128]{1,0:T(8,128)(2,1)S(1)} %collective-permute-done.32.refs_20_), channel_id=1, source_target_pairs={{0,8},{2,10},{4,12},{6,14},{8,0},{10,2},{12,4},{14,6},{16,24},{18,... | collective-permute-start | bytes 786440 | tf_op jit(solution)/shard_map/ppermute | solution.py:345
  37.9 8.1 %collective-permute-done.24.refs_12_ = bf16[1024,256]{1,0:T(8,128)(2,1)S(1)} collective-permute-done((bf16[1024,256]{1,0:T(8,128)(2,1)S(1)}, bf16[1024,256]{1,0:T(8,128)(2,1)S(1)}, u32[]{:S(2)}, u32[]{:S(2)}) %collective-permute-start.24) | collective-permute-done | bytes 524320 | tf_op jit(solution)/shard_map/ppermute | solution.py:371
  46.6 5.3 %collective-permute-start.4 = (bf16[288,512]{1,0:T(8,128)(2,1)S(1)}, bf16[288,512]{1,0:T(8,128)(2,1)S(1)}, u32[]{:S(2)}, u32[]{:S(2)}) collective-permute-start(bf16[288,512]{1,0:T(8,128)(2,1)S(1)} %collective-permute-done.refs_7_), channel_id=1, source_target_pairs={{0,4},{2,6},{4,0},{6,2},{8,12},{10,14},{12,8},{14,10},{16,20},{18,... | collective-permute-start | bytes 884744 | tf_op jit(solution)/shard_map/ppermute | solution.py:345
  53.7 2.7 %collective-permute-start.18 = (bf16[1024,128]{1,0:T(8,128)(2,1)S(1)}, bf16[1024,128]{1,0:T(8,128)(2,1)S(1)}, u32[]{:S(2)}, u32[]{:S(2)}) collective-permute-start(bf16[1024,128]{1,0:T(8,128)(2,1)S(1)} %collective-permute-done.14.refs_2_), channel_id=1, source_target_pairs={{0,4},{2,6},{4,0},{6,2},{8,12},{10,14},{12,8},{14,10},{16,20},{18,... | collective-permute-start | bytes 786440 | tf_op jit(solution)/shard_map/ppermute | solution.py:345
  56.5 2.5 %begin.1 = (bf16[8,256,256]{2,1,0:T(8,128)(2,1)S(1)}, bf16[1024,512]{1,0:T(8,128)(2,1)S(1)}, f32[16,256]{1,0:T(8,128)S(1)}, f32[8,128,256]{2,1,0:T(8,128)S(1)}) custom-call(bf16[256,1024]{1,0:T(8,128)(2,1)S(1)} %copy-done.4, f32[1,1024]{1,0:T(1,128)S(1)} %bitcast.7, bf16[1024,1024]{1,0:T(8,128)(2,1)S(1)} %copy-done, bf16[1024,512]{1,0:T(8,128)(2,1)S(1)} %copy-done.1, ...), custom_call_target="tpu_custom_call" | custom-call | flops 2000000000 | bytes 6000000 | tf_op jit(solution)/shard_map/begin/pallas_call | solution.py:385
  60.3 10.3 %collective-permute-done.18.refs_6_ = bf16[1024,128]{1,0:T(8,128)(2,1)S(1)} collective-permute-done((bf16[1024,128]{1,0:T(8,128)(2,1)S(1)}, bf16[1024,128]{1,0:T(8,128)(2,1)S(1)}, u32[]{:S(2)}, u32[]{:S(2)}) %collective-permute-start.18) | collective-permute-done | bytes 262176 | tf_op jit(solution)/shard_map/ppermute | solution.py:345
  71.9 4.0 %collective-permute-start.22 = (bf16[1024,256]{1,0:T(8,128)(2,1)S(1)}, bf16[1024,256]{1,0:T(8,128)(2,1)S(1)}, u32[]{:S(2)}, u32[]{:S(2)}) collective-permute-start(bf16[1024,256]{1,0:T(8,128)(2,1)S(1)} %collective-permute-done.20.refs_8_), channel_id=1, source_target_pairs={{0,8},{2,10},{4,12},{6,14},{8,0},{10,2},{12,4},{14,6},{16,24},{18,... | collective-permute-start | bytes 1572872 | tf_op jit(solution)/shard_map/ppermute | solution.py:345
  81.5 6.4 %collective-permute-done.22.refs_10_ = bf16[1024,256]{1,0:T(8,128)(2,1)S(1)} collective-permute-done((bf16[1024,256]{1,0:T(8,128)(2,1)S(1)}, bf16[1024,256]{1,0:T(8,128)(2,1)S(1)}, u32[]{:S(2)}, u32[]{:S(2)}) %collective-permute-start.22) | collective-permute-done | bytes 524320 | tf_op jit(solution)/shard_map/ppermute | solution.py:345
  88.8 1.7 %collective-permute-done.26.refs_14_ = bf16[1024,256]{1,0:T(8,128)(2,1)S(1)} collective-permute-done((bf16[1024,256]{1,0:T(8,128)(2,1)S(1)}, bf16[1024,256]{1,0:T(8,128)(2,1)S(1)}, u32[]{:S(2)}, u32[]{:S(2)}) %collective-permute-start.26) | collective-permute-done | bytes 524320 | tf_op jit(solution)/shard_map/ppermute | solution.py:345
  90.6 1.5 %collective-permute-start.11 = (bf16[256,1024]{1,0:T(8,128)(2,1)S(1)}, bf16[256,1024]{1,0:T(8,128)(2,1)S(1)}, u32[]{:S(2)}, u32[]{:S(2)}) collective-permute-start(bf16[256,1024]{1,0:T(8,128)(2,1)S(1)} %finish.1.rows_ref), channel_id=1, source_target_pairs={{0,1},{1,0},{2,3},{3,2},{4,5},{5,4},{6,7},{7,6},{8,9},{9,8},{10,11... | collective-permute-start | bytes 1572872 | tf_op jit(solution)/shard_map/ppermute | solution.py:443
  92.1 3.5 %ours.1.ours_ref = bf16[256,4096]{1,0:T(8,128)(2,1)S(1)} custom-call(bf16[256,1024]{1,0:T(8,128)(2,1)S(1)} %finish.1.rows_ref, bf16[1024,4096]{1,0:T(8,128)(2,1)S(1)} %bitcast.5), custom_call_target="tpu_custom_call" | custom-call | flops 2000000000 | bytes 10000000 | tf_op jit(solution)/shard_map/ours/pallas_call | solution.py:444
  95.7 9.1 %collective-permute-done.11.rows_ref = bf16[256,1024]{1,0:T(8,128)(2,1)S(1)} collective-permute-done((bf16[256,1024]{1,0:T(8,128)(2,1)S(1)}, bf16[256,1024]{1,0:T(8,128)(2,1)S(1)}, u32[]{:S(2)}, u32[]{:S(2)}) %collective-permute-start.11) | collective-permute-done | bytes 524320 | tf_op jit(solution)/shard_map/ppermute | solution.py:443
  104.8 3.5 %shard_map.113 = bf16[256,4096]{1,0:T(8,128)(2,1)} custom-call(bf16[256,1024]{1,0:T(8,128)(2,1)S(1)} %collective-permute-done.11.rows_ref, bf16[256,4096]{1,0:T(8,128)(2,1)S(1)} %ours.1.ours_ref, bf16[1024,128]{1,0:T(8,128)(2,1)S(1)} %collective-permute-done.12.refs_0_, bf16[1024,128]{1,0:T(8,128)(2,1)S(1)} %collective-permute-done.13.refs_1_, ...), custom_call_target="tpu_custom_call" | custom-call | flops 1000000000 | bytes 5000000 | tf_op jit(solution)/shard_map/pallas_call | solution.py:462
  (90 shorter events, 15.8 us)
Async XLA Ops:
  2.8 12.8 %collective-permute-start.12 = (bf16[1024,128]{1,0:T(8,128)(2,1)}, bf16[1024,128]{1,0:T(8,128)(2,1)S(1)}, u32[]{:S(2)}, u32[]{:S(2)}) collective-permute-start(bf16[1024,128]{1,0:T(8,128)(2,1)} %get-tuple-element.34), channel_id=1, source_target_pairs={{0,1},{1,0},{2,3},{3,2},{4,5},{5,4},{6,7},{7,6},{8,9},{9,8},{10,11... | collective-permute-start | bytes 786440 | tf_op jit(solution)/shard_map/ppermute | solution.py:371
  5.8 13.0 %collective-permute-start.28 = (bf16[1024,128]{1,0:T(8,128)(2,1)}, bf16[1024,128]{1,0:T(8,128)(2,1)S(1)}, u32[]{:S(2)}, u32[]{:S(2)}) collective-permute-start(bf16[1024,128]{1,0:T(8,128)(2,1)} %get-tuple-element.37), channel_id=1, source_target_pairs={{0,1},{1,0},{2,3},{3,2},{4,5},{5,4},{6,7},{7,6},{8,9},{9,8},{10,11... | collective-permute-start | bytes 786440 | tf_op jit(solution)/shard_map/ppermute | solution.py:371
  5.9 18.5 %collective-permute-start.32 = (bf16[1024,128]{1,0:T(8,128)(2,1)}, bf16[1024,128]{1,0:T(8,128)(2,1)S(1)}, u32[]{:S(2)}, u32[]{:S(2)}) collective-permute-start(bf16[1024,128]{1,0:T(8,128)(2,1)} %get-tuple-element.38), channel_id=1, source_target_pairs={{0,1},{1,0},{2,3},{3,2},{4,5},{5,4},{6,7},{7,6},{8,9},{9,8},{10,11... | collective-permute-start | bytes 786440 | tf_op jit(solution)/shard_map/ppermute | solution.py:371
  8.4 16.1 %collective-permute-start = (bf16[288,512]{1,0:T(8,128)(2,1)S(1)}, bf16[288,512]{1,0:T(8,128)(2,1)S(1)}, u32[]{:S(2)}, u32[]{:S(2)}) collective-permute-start(bf16[288,512]{1,0:T(8,128)(2,1)S(1)} %pack.1.refs_7_), channel_id=1, source_target_pairs={{0,8},{2,10},{4,12},{6,14},{8,16},{10,18},{12,20},{14,22},{16,24},... | collective-permute-start | bytes 884744 | tf_op jit(solution)/shard_map/ppermute | solution.py:345
  12.2 14.4 %collective-permute-start.7 = (bf16[288,512]{1,0:T(8,128)(2,1)S(1)}, bf16[288,512]{1,0:T(8,128)(2,1)S(1)}, u32[]{:S(2)}, u32[]{:S(2)}) collective-permute-start(bf16[288,512]{1,0:T(8,128)(2,1)S(1)} %pack.1.refs_7_), channel_id=1, source_target_pairs={{0,4},{2,6},{8,12},{10,14},{16,20},{18,22},{24,28},{26,30},{1,5},{... | collective-permute-start | bytes 884744 | tf_op jit(solution)/shard_map/ppermute | solution.py:345
  15.6 20.9 %collective-permute-start.20 = (bf16[1024,256]{1,0:T(8,128)(2,1)S(1)}, bf16[1024,256]{1,0:T(8,128)(2,1)S(1)}, u32[]{:S(2)}, u32[]{:S(2)}) collective-permute-start(bf16[1024,256]{1,0:T(8,128)(2,1)S(1)} %copy-done.11), channel_id=1, source_target_pairs={{0,1},{1,0},{2,3},{3,2},{4,5},{5,4},{6,7},{7,6},{8,9},{9,8},{10,11... | collective-permute-start | bytes 1572872 | tf_op jit(solution)/shard_map/ppermute | solution.py:371
  18.8 27.2 %collective-permute-start.24 = (bf16[1024,256]{1,0:T(8,128)(2,1)S(1)}, bf16[1024,256]{1,0:T(8,128)(2,1)S(1)}, u32[]{:S(2)}, u32[]{:S(2)}) collective-permute-start(bf16[1024,256]{1,0:T(8,128)(2,1)S(1)} %copy-done.10), channel_id=1, source_target_pairs={{0,1},{1,0},{2,3},{3,2},{4,5},{5,4},{6,7},{7,6},{8,9},{9,8},{10,11... | collective-permute-start | bytes 1572872 | tf_op jit(solution)/shard_map/ppermute | solution.py:371
  24.5 9.3 %collective-permute-start.14 = (bf16[1024,128]{1,0:T(8,128)(2,1)S(1)}, bf16[1024,128]{1,0:T(8,128)(2,1)S(1)}, u32[]{:S(2)}, u32[]{:S(2)}) collective-permute-start(bf16[1024,128]{1,0:T(8,128)(2,1)S(1)} %collective-permute-done.12.refs_0_), channel_id=1, source_target_pairs={{0,8},{2,10},{4,12},{6,14},{8,0},{10,2},{12,4},{14,6},{16,24},{18,... | collective-permute-start | bytes 786440 | tf_op jit(solution)/shard_map/ppermute | solution.py:345
  28.1 18.0 %collective-permute-start.30 = (bf16[1024,128]{1,0:T(8,128)(2,1)S(1)}, bf16[1024,128]{1,0:T(8,128)(2,1)S(1)}, u32[]{:S(2)}, u32[]{:S(2)}) collective-permute-start(bf16[1024,128]{1,0:T(8,128)(2,1)S(1)} %collective-permute-done.28.refs_16_), channel_id=1, source_target_pairs={{0,8},{2,10},{4,12},{6,14},{8,0},{10,2},{12,4},{14,6},{16,24},{18,... | collective-permute-start | bytes 786440 | tf_op jit(solution)/shard_map/ppermute | solution.py:345
  33.7 18.7 %collective-permute-start.1 = (bf16[288,512]{1,0:T(8,128)(2,1)S(1)}, bf16[288,512]{1,0:T(8,128)(2,1)S(1)}, u32[]{:S(2)}, u32[]{:S(2)}) collective-permute-start(bf16[288,512]{1,0:T(8,128)(2,1)S(1)} %collective-permute-done.refs_7_), channel_id=1, source_target_pairs={{2,10},{4,12},{6,14},{10,18},{12,20},{14,22},{18,26},{20,28},{22,3... | collective-permute-start | bytes 884744 | tf_op jit(solution)/shard_map/ppermute | solution.py:345
  35.0 11.6 %collective-permute-start.34 = (bf16[1024,128]{1,0:T(8,128)(2,1)S(1)}, bf16[1024,128]{1,0:T(8,128)(2,1)S(1)}, u32[]{:S(2)}, u32[]{:S(2)}) collective-permute-start(bf16[1024,128]{1,0:T(8,128)(2,1)S(1)} %collective-permute-done.32.refs_20_), channel_id=1, source_target_pairs={{0,8},{2,10},{4,12},{6,14},{8,0},{10,2},{12,4},{14,6},{16,24},{18,... | collective-permute-start | bytes 786440 | tf_op jit(solution)/shard_map/ppermute | solution.py:345
  36.5 15.4 %collective-permute-start.13 = (bf16[1024,128]{1,0:T(8,128)(2,1)S(1)}, bf16[1024,128]{1,0:T(8,128)(2,1)S(1)}, u32[]{:S(2)}, u32[]{:S(2)}) collective-permute-start(bf16[1024,128]{1,0:T(8,128)(2,1)S(1)} %collective-permute-done.12.refs_0_), channel_id=1, source_target_pairs={{0,2},{2,0},{4,6},{6,4},{8,10},{10,8},{12,14},{14,12},{16,18},{18,... | collective-permute-start | bytes 786440 | tf_op jit(solution)/shard_map/ppermute | solution.py:345
  46.6 13.1 %collective-permute-start.4 = (bf16[288,512]{1,0:T(8,128)(2,1)S(1)}, bf16[288,512]{1,0:T(8,128)(2,1)S(1)}, u32[]{:S(2)}, u32[]{:S(2)}) collective-permute-start(bf16[288,512]{1,0:T(8,128)(2,1)S(1)} %collective-permute-done.refs_7_), channel_id=1, source_target_pairs={{0,4},{2,6},{4,0},{6,2},{8,12},{10,14},{12,8},{14,10},{16,20},{18,... | collective-permute-start | bytes 884744 | tf_op jit(solution)/shard_map/ppermute | solution.py:345
  52.4 18.2 %collective-permute-start.2 = (bf16[288,512]{1,0:T(8,128)(2,1)S(1)}, bf16[288,512]{1,0:T(8,128)(2,1)S(1)}, u32[]{:S(2)}, u32[]{:S(2)}) collective-permute-start(bf16[288,512]{1,0:T(8,128)(2,1)S(1)} %collective-permute-done.1), channel_id=1, source_target_pairs={{4,0},{6,2},{12,8},{14,10},{20,16},{22,18},{28,24},{30,26},{5,1},{... | collective-permute-start | bytes 884744 | tf_op jit(solution)/shard_map/ppermute | solution.py:345
  53.7 16.9 %collective-permute-start.18 = (bf16[1024,128]{1,0:T(8,128)(2,1)S(1)}, bf16[1024,128]{1,0:T(8,128)(2,1)S(1)}, u32[]{:S(2)}, u32[]{:S(2)}) collective-permute-start(bf16[1024,128]{1,0:T(8,128)(2,1)S(1)} %collective-permute-done.14.refs_2_), channel_id=1, source_target_pairs={{0,4},{2,6},{4,0},{6,2},{8,12},{10,14},{12,8},{14,10},{16,20},{18,... | collective-permute-start | bytes 786440 | tf_op jit(solution)/shard_map/ppermute | solution.py:345
  59.7 12.1 %collective-permute-start.15 = (bf16[1024,128]{1,0:T(8,128)(2,1)S(1)}, bf16[1024,128]{1,0:T(8,128)(2,1)S(1)}, u32[]{:S(2)}, u32[]{:S(2)}) collective-permute-start(bf16[1024,128]{1,0:T(8,128)(2,1)S(1)} %collective-permute-done.14.refs_2_), channel_id=1, source_target_pairs={{0,2},{2,0},{4,6},{6,4},{8,10},{10,8},{12,14},{14,12},{16,18},{18,... | collective-permute-start | bytes 786440 | tf_op jit(solution)/shard_map/ppermute | solution.py:345
  59.7 16.1 %collective-permute-start.17 = (bf16[1024,128]{1,0:T(8,128)(2,1)S(1)}, bf16[1024,128]{1,0:T(8,128)(2,1)S(1)}, u32[]{:S(2)}, u32[]{:S(2)}) collective-permute-start(bf16[1024,128]{1,0:T(8,128)(2,1)S(1)} %collective-permute-done.16.refs_4_), channel_id=1, source_target_pairs={{0,2},{2,0},{4,6},{6,4},{8,10},{10,8},{12,14},{14,12},{16,18},{18,... | collective-permute-start | bytes 786440 | tf_op jit(solution)/shard_map/ppermute | solution.py:345
  60.2 18.5 %collective-permute-start.6 = (bf16[288,512]{1,0:T(8,128)(2,1)S(1)}, bf16[288,512]{1,0:T(8,128)(2,1)S(1)}, u32[]{:S(2)}, u32[]{:S(2)}) collective-permute-start(bf16[288,512]{1,0:T(8,128)(2,1)S(1)} %collective-permute-done.1), channel_id=1, source_target_pairs={{0,2},{2,0},{4,6},{6,4},{8,10},{10,8},{12,14},{14,12},{16,18},{18,... | collective-permute-start | bytes 884744 | tf_op jit(solution)/shard_map/ppermute | solution.py:345
  71.9 16.0 %collective-permute-start.22 = (bf16[1024,256]{1,0:T(8,128)(2,1)S(1)}, bf16[1024,256]{1,0:T(8,128)(2,1)S(1)}, u32[]{:S(2)}, u32[]{:S(2)}) collective-permute-start(bf16[1024,256]{1,0:T(8,128)(2,1)S(1)} %collective-permute-done.20.refs_8_), channel_id=1, source_target_pairs={{0,8},{2,10},{4,12},{6,14},{8,0},{10,2},{12,4},{14,6},{16,24},{18,... | collective-permute-start | bytes 1572872 | tf_op jit(solution)/shard_map/ppermute | solution.py:345
  75.9 14.6 %collective-permute-start.26 = (bf16[1024,256]{1,0:T(8,128)(2,1)S(1)}, bf16[1024,256]{1,0:T(8,128)(2,1)S(1)}, u32[]{:S(2)}, u32[]{:S(2)}) collective-permute-start(bf16[1024,256]{1,0:T(8,128)(2,1)S(1)} %collective-permute-done.24.refs_12_), channel_id=1, source_target_pairs={{0,4},{2,6},{4,0},{6,2},{8,12},{10,14},{12,8},{14,10},{16,20},{18,... | collective-permute-start | bytes 1572872 | tf_op jit(solution)/shard_map/ppermute | solution.py:345
  78.8 11.7 %collective-permute-start.19 = (bf16[1024,128]{1,0:T(8,128)(2,1)S(1)}, bf16[1024,128]{1,0:T(8,128)(2,1)S(1)}, u32[]{:S(2)}, u32[]{:S(2)}) collective-permute-start(bf16[1024,128]{1,0:T(8,128)(2,1)S(1)} %collective-permute-done.18.refs_6_), channel_id=1, source_target_pairs={{0,2},{2,0},{4,6},{6,4},{8,10},{10,8},{12,14},{14,12},{16,18},{18,... | collective-permute-start | bytes 786440 | tf_op jit(solution)/shard_map/ppermute | solution.py:345
  80.9 14.7 %collective-permute-start.21 = (bf16[1024,256]{1,0:T(8,128)(2,1)S(1)}, bf16[1024,256]{1,0:T(8,128)(2,1)S(1)}, u32[]{:S(2)}, u32[]{:S(2)}) collective-permute-start(bf16[1024,256]{1,0:T(8,128)(2,1)S(1)} %collective-permute-done.20.refs_8_), channel_id=1, source_target_pairs={{0,2},{2,0},{4,6},{6,4},{8,10},{10,8},{12,14},{14,12},{16,18},{18,... | collective-permute-start | bytes 1572872 | tf_op jit(solution)/shard_map/ppermute | solution.py:345
  81.1 14.6 %collective-permute-start.25 = (bf16[1024,256]{1,0:T(8,128)(2,1)S(1)}, bf16[1024,256]{1,0:T(8,128)(2,1)S(1)}, u32[]{:S(2)}, u32[]{:S(2)}) collective-permute-start(bf16[1024,256]{1,0:T(8,128)(2,1)S(1)} %collective-permute-done.24.refs_12_), channel_id=1, source_target_pairs={{0,2},{2,0},{4,6},{6,4},{8,10},{10,8},{12,14},{14,12},{16,18},{18,... | collective-permute-start | bytes 1572872 | tf_op jit(solution)/shard_map/ppermute | solution.py:345
  90.6 14.2 %collective-permute-start.11 = (bf16[256,1024]{1,0:T(8,128)(2,1)S(1)}, bf16[256,1024]{1,0:T(8,128)(2,1)S(1)}, u32[]{:S(2)}, u32[]{:S(2)}) collective-permute-start(bf16[256,1024]{1,0:T(8,128)(2,1)S(1)} %finish.1.rows_ref), channel_id=1, source_target_pairs={{0,1},{1,0},{2,3},{3,2},{4,5},{5,4},{6,7},{7,6},{8,9},{9,8},{10,11... | collective-permute-start | bytes 1572872 | tf_op jit(solution)/shard_map/ppermute | solution.py:443
  (26 other events, 480.7 us)
